TPU v7x, 256 devices: a whole 4x4x8 slice. The times are simulated.
256 devices in a mesh: ra: 16 (over y, x), cb: 16 (over z, core).
Axes of the slice: x: 4, y: 4, z: 8, core: 2. Of those that a mesh axis runs over, the one named last changes fastest.
Arguments:
- hidden_states: bfloat16 [384, 4096], P(None, 'ra'), may hold values from -40 to 40
- gain_first: bfloat16 [4096], P('ra'), may hold values from 0.099609375 to 1.8984375
- gate_first: bfloat16 [4096, 11264], P('ra', 'cb'), may hold values from -0.09375 to 0.09375
- up_first: bfloat16 [4096, 11264], P('ra', 'cb'), may hold values from -0.09375 to 0.09375
- down_first: bfloat16 [11264, 4096], P('cb', 'ra'), may hold values from -0.0546875 to 0.0546875
- gain_second: bfloat16 [4096], P('ra'), may hold values from 0.099609375 to 1.8984375
- gate_second: bfloat16 [4096, 11264], P('ra', 'cb'), may hold values from -0.09375 to 0.09375
- up_second: bfloat16 [4096, 11264], P('ra', 'cb'), may hold values from -0.09375 to 0.09375
- down_second: bfloat16 [11264, 4096], P('cb', 'ra'), may hold values from -0.0546875 to 0.0546875
- gain_last: bfloat16 [4096], P('ra'), may hold values from 0.099609375 to 1.8984375
Outputs:
- closed: bfloat16 [384, 4096], P(None, 'ra')
All inputs are finite; a program needn't handle non-finite values.
Results may differ from a plain program's by a relative error of at most 0.0098.
Values may be sent and summed in bfloat16 or wider, within the bound.
No kernel may reach another device: no remote copies, remote signals or barrier semaphores. Data moves between devices by JAX's collectives and lax.ppermute only.
A program may use at most 64 MiB of HBM per device.

v0:
```python
import jax
import jax.numpy as jnp
from jax import lax
from jax.sharding import Mesh
from jax.sharding import PartitionSpec as P

D = 4096
RA = ("ra_0", "ra_1")


norm_eps = 1e-06
residual_weight = 0.25
branch_weight = 0.5


def in_blocks(value, dim, length):
    before, after = (value.shape[:dim], value.shape[dim + 1 :])
    return jnp.moveaxis(value.reshape(*before, length, -1, *after), dim, 0)


def sum_at_owner(value, axis, dim):
    length = lax.axis_size(axis)
    blocks = lax.all_to_all(in_blocks(value, dim, length), axis, 0, 0, tiled=True)
    return jnp.sum(blocks, axis=0)


def sent_together(arrays, axis, dim, along):
    widths = [a.shape[along] for a in arrays]
    both = jnp.concatenate(arrays, axis=along)
    filled = sum_at_owner(both, axis, dim)
    return tuple(jnp.split(filled, [sum(widths[:k]) for k in range(1, len(widths))], axis=along))


def from_everyone(value, axis):
    length = lax.axis_size(axis)
    return lax.all_to_all(
        jnp.broadcast_to(value[None], (length, *value.shape)), axis, 0, 0, tiled=True
    )


def laid_out(blocks, dim):
    shape = list(blocks.shape[1:])
    shape[dim] *= blocks.shape[0]
    return jnp.moveaxis(blocks, 0, dim).reshape(shape)


def gather_directly(value, axis, dim):
    blocks = from_everyone(value, axis)
    return laid_out(blocks, dim)


def over_axes(value, axes):
    for axis in axes:
        value = lax.psum(value, axis)
    return value


def half_step(stream, gain, w_gate, w_up, w_down):
    values = stream.astype(jnp.float32)
    local_squares = jnp.sum(values * values, axis=1)
    normed = (values * gain.astype(jnp.float32)).astype(jnp.bfloat16)
    gate_part = jnp.dot(normed, w_gate, preferred_element_type=jnp.float32)
    upper_part = jnp.dot(normed, w_up, preferred_element_type=jnp.float32)
    gate, upper, squares = sent_together((gate_part, upper_part, local_squares[:, None]), RA, 0, 1)
    scale = lax.rsqrt(squares / D + norm_eps)
    hidden = (jax.nn.silu(gate * scale) * (upper * scale)).astype(jnp.bfloat16)
    branch = jnp.dot(gather_directly(hidden, RA, 0), w_down, preferred_element_type=jnp.float32)
    block = sum_at_owner(branch, "cb", 0)
    count = block.shape[0]
    offset = lax.axis_index("cb") * count
    own_rows = lax.dynamic_slice_in_dim(values, offset, count, 0)
    updated = (residual_weight * own_rows + branch_weight * block).astype(jnp.bfloat16)
    return gather_directly(updated, "cb", 0)


def body(
    hidden_states,
    gain_first,
    gate_first,
    up_first,
    down_first,
    gain_second,
    gate_second,
    up_second,
    down_second,
    gain_last,
):
    first = half_step(hidden_states, gain_first, gate_first, up_first, down_first)
    second = half_step(first, gain_second, gate_second, up_second, down_second)
    values = second.astype(jnp.float32)
    squares = over_axes(jnp.sum(values * values, axis=1), RA)
    scale = lax.rsqrt(squares / D + norm_eps)[:, None]
    return (values * scale * gain_last.astype(jnp.float32)).astype(jnp.bfloat16)


def solution(mesh):
    split = Mesh(mesh.devices.reshape(4, 4, mesh.shape["cb"]), ("ra_0", "ra_1", "cb"))
    return jax.shard_map(
        body,
        mesh=split,
        in_specs=(
            P(None, RA),
            P(RA),
            P(RA, "cb"),
            P(RA, "cb"),
            P("cb", RA),
            P(RA),
            P(RA, "cb"),
            P(RA, "cb"),
            P("cb", RA),
            P(RA),
        ),
        out_specs=P(None, RA),
        check_vma=False,
    )
```

profile of v0, /device:TPU:1, one launch (start us, length us, event | category | flops | bytes accessed | tf_op | source)
XLA Modules:
  0.0 209.0 jit_solution(11229459971690430254)
XLA Ops:
  0.0 0.0 copy-start
  0.0 0.7 convert_element_type.56
  0.7 1.1 multiply_reduce_fusion.2
  1.8 0.0 copy-done
  1.8 2.3 %fusion.11 = f32[384,704]{1,0:T(8,128)} fusion(bf16[256,704]{0,1:T(8,128)(2,1)S(1)} %copy-done, f32[256]{0:T(256)S(1)} %convert_element_type.56, bf16[384,256]{1,0:T(8,128)(2,1)} %param.10), kind=kOutput, calls=%fused_computation.17 | convolution fusion | flops 138706944 | bytes 1639424 | tf_op jit(solution)/shard_map/dot_general | solution.py:62
  4.1 0.0 copy-done.1
  4.1 0.0 copy-done.2
  4.1 1.4 fusion.10
  5.5 0.2 concatenate.22
  5.7 2.7 %concatenate.19 = f32[16,24,1409]{2,1,0:T(8,128)S(1)} concatenate(f32[16,24,704]{2,1,0:T(8,128)} %bitcast.28, f32[16,24,704]{2,1,0:T(8,128)} %bitcast.29, f32[16,24,1]{2,1,0:T(8,128)S(1)} %concatenate.22), dimensions={2} | concatenate | bytes 4328448 | tf_op jit(solution)/shard_map/concatenate | solution.py:29
  8.5 37.9 %all_to_all.40 = f32[16,24,1409]{2,1,0:T(8,128)} all-to-all(f32[16,24,1409]{2,1,0:T(8,128)S(1)} %concatenate.19), channel_id=1, replica_groups=mesh['ra_0'=4,'ra_1'=4,'cb'=16] {'ra_0','ra_1'}, dimensions={0} | all-to-all | bytes 4328448 | tf_op jit(solution)/shard_map/all_to_all | solution.py:23
  46.3 1.8 reduce_sum.66
  48.1 0.0 copy-start.3
  48.1 0.1 fusion.21
  48.3 0.1 fusion.15
  48.4 14.2 %all_to_all.41 = bf16[16,24,704]{2,1,0:T(8,128)(2,1)S(1)} all-to-all(bf16[16,24,704]{2,1,0:T(8,128)(2,1)S(1)} %broadcast_in_dim.8), channel_id=1, replica_groups=mesh['ra_0'=4,'ra_1'=4,'cb'=16] {'ra_0','ra_1'}, dimensions={0} | all-to-all | bytes 1081344 | tf_op jit(solution)/shard_map/all_to_all | solution.py:36
  62.7 0.0 copy-done.3
  62.7 1.1 fusion.8
  63.7 10.7 %all-to-all-start.2 = ((f32[16,24,256]{2,1,0:T(8,128)}), f32[16,24,256]{2,1,0:T(8,128)S(1)}, u32[]{:S(2)}, u32[]{:S(2)}) async-start(f32[16,24,256]{2,1,0:T(8,128)} %fusion.8), calls=%async_computation.2 | async-start | bytes 786432 | tf_op jit(solution)/shard_map/all_to_all | solution.py:23
  74.5 14.4 %all-to-all-done.2 = f32[16,24,256]{2,1,0:T(8,128)S(1)} async-done(((f32[16,24,256]{2,1,0:T(8,128)}), f32[16,24,256]{2,1,0:T(8,128)S(1)}, u32[]{:S(2)}, u32[]{:S(2)}) %all-to-all-start.2) | async-done | bytes 393248 | tf_op jit(solution)/shard_map/all_to_all | solution.py:23
  89.0 0.7 broadcast_in_dim.9
  89.7 3.6 %all-to-all-start.3 = ((bf16[16,24,256]{2,1,0:T(8,128)(2,1)}), bf16[16,24,256]{2,1,0:T(8,128)(2,1)S(1)}, u32[]{:S(2)}, u32[]{:S(2)}) async-start(bf16[16,24,256]{2,1,0:T(8,128)(2,1)} %broadcast_in_dim.9), calls=%async_computation.3 | async-start | bytes 393216 | tf_op jit(solution)/shard_map/all_to_all | solution.py:36
  93.3 0.0 copy-done.7
  93.3 9.6 %all-to-all-done.3 = bf16[16,24,256]{2,1,0:T(8,128)(2,1)S(1)} async-done(((bf16[16,24,256]{2,1,0:T(8,128)(2,1)}), bf16[16,24,256]{2,1,0:T(8,128)(2,1)S(1)}, u32[]{:S(2)}, u32[]{:S(2)}) %all-to-all-start.3) | async-done | bytes 196640 | tf_op jit(solution)/shard_map/all_to_all | solution.py:36
  102.9 0.1 multiply_reduce_fusion.1
  103.0 0.2 copy.31
  103.2 0.0 copy-done.4
  103.2 1.4 fusion.4
  104.6 0.0 copy-done.5
  104.6 1.4 fusion.6
  106.0 2.7 %concatenate.21 = f32[16,24,1409]{2,1,0:T(8,128)S(1)} concatenate(f32[16,24,704]{2,1,0:T(8,128)} %fusion.6, f32[16,24,704]{2,1,0:T(8,128)} %fusion.4, f32[16,24,1]{2,1,0:T(8,128)S(1)} %copy.31), dimensions={2} | concatenate | bytes 4328448 | tf_op jit(solution)/shard_map/concatenate | solution.py:29
  108.7 34.5 %all_to_all.42 = f32[16,24,1409]{2,1,0:T(8,128)} all-to-all(f32[16,24,1409]{2,1,0:T(8,128)S(1)} %concatenate.21), channel_id=1, replica_groups=mesh['ra_0'=4,'ra_1'=4,'cb'=16] {'ra_0','ra_1'}, dimensions={0} | all-to-all | bytes 4328448 | tf_op jit(solution)/shard_map/all_to_all | solution.py:23
  143.2 1.8 reduce_sum.69
  145.0 0.0 copy-start.6
  145.0 0.1 fusion.18
  145.1 0.1 fusion.13
  145.3 14.0 %all_to_all.43 = bf16[16,24,704]{2,1,0:T(8,128)(2,1)S(1)} all-to-all(bf16[16,24,704]{2,1,0:T(8,128)(2,1)S(1)} %broadcast_in_dim.10), channel_id=1, replica_groups=mesh['ra_0'=4,'ra_1'=4,'cb'=16] {'ra_0','ra_1'}, dimensions={0} | all-to-all | bytes 1081344 | tf_op jit(solution)/shard_map/all_to_all | solution.py:36
  159.3 1.1 fusion.2
  160.3 5.5 %all-to-all-start.6 = ((f32[16,24,256]{2,1,0:T(8,128)}), f32[16,24,256]{2,1,0:T(8,128)S(1)}, u32[]{:S(2)}, u32[]{:S(2)}) async-start(f32[16,24,256]{2,1,0:T(8,128)} %fusion.2), calls=%async_computation.6 | async-start | bytes 786432 | tf_op jit(solution)/shard_map/all_to_all | solution.py:23
  165.9 14.5 %all-to-all-done.6 = f32[16,24,256]{2,1,0:T(8,128)S(1)} async-done(((f32[16,24,256]{2,1,0:T(8,128)}), f32[16,24,256]{2,1,0:T(8,128)S(1)}, u32[]{:S(2)}, u32[]{:S(2)}) %all-to-all-start.6) | async-done | bytes 393248 | tf_op jit(solution)/shard_map/all_to_all | solution.py:23
  180.4 0.7 broadcast_in_dim.11
  181.1 3.4 %all-to-all-start.7 = ((bf16[16,24,256]{2,1,0:T(8,128)(2,1)}), bf16[16,24,256]{2,1,0:T(8,128)(2,1)S(1)}, u32[]{:S(2)}, u32[]{:S(2)}) async-start(bf16[16,24,256]{2,1,0:T(8,128)(2,1)} %broadcast_in_dim.11), calls=%async_computation.7 | async-start | bytes 393216 | tf_op jit(solution)/shard_map/all_to_all | solution.py:36
  184.6 9.6 %all-to-all-done.7 = bf16[16,24,256]{2,1,0:T(8,128)(2,1)S(1)} async-done(((bf16[16,24,256]{2,1,0:T(8,128)(2,1)}), bf16[16,24,256]{2,1,0:T(8,128)(2,1)S(1)}, u32[]{:S(2)}, u32[]{:S(2)}) %all-to-all-start.7) | async-done | bytes 196640 | tf_op jit(solution)/shard_map/all_to_all | solution.py:36
  194.2 0.1 multiply_reduce_fusion
  194.3 0.1 reduce_sum.72
  194.4 6.8 %psum.14 = f32[384]{0:T(512)S(1)} all-reduce(f32[384]{0:T(512)S(1)} %reduce_sum.72), channel_id=1, replica_groups=mesh['ra_0'=4,'ra_1'=4,'cb'=16] {'ra_0'}, use_global_device_ids=true, to_apply=%region_7.8 | all-reduce | flops 384 | bytes 3072 | tf_op jit(solution)/shard_map/psum | solution.py:54
  201.2 6.9 %psum.15 = f32[384]{0:T(512)S(1)} all-reduce(f32[384]{0:T(512)S(1)} %psum.14), channel_id=1, replica_groups=mesh['ra_0'=4,'ra_1'=4,'cb'=16] {'ra_1'}, use_global_device_ids=true, to_apply=%region_8.9 | all-reduce | flops 384 | bytes 3072 | tf_op jit(solution)/shard_map/psum | solution.py:54
  208.2 0.8 fusion.1
  (19 shorter events, 0.3 us)
Async XLA Ops:
  0.0 1.8 copy-start
  0.0 4.1 %copy-start.1 = (bf16[384,256]{1,0:T(8,128)(2,1)S(1)}, bf16[384,256]{1,0:T(8,128)(2,1)}, u32[]{:S(2)}) copy-start(bf16[384,256]{1,0:T(8,128)(2,1)} %param.10) | copy-start | bytes 589828
  0.0 4.1 %copy-start.2 = (bf16[256,704]{0,1:T(8,128)(2,1)S(1)}, bf16[256,704]{0,1:T(8,128)(2,1)}, u32[]{:S(2)}) copy-start(bf16[256,704]{0,1:T(8,128)(2,1)} %param.13) | copy-start | bytes 1081348
  48.1 14.5 %copy-start.3 = (bf16[704,256]{1,0:T(8,128)(2,1)S(1)}, bf16[704,256]{1,0:T(8,128)(2,1)}, u32[]{:S(2)}) copy-start(bf16[704,256]{1,0:T(8,128)(2,1)} %param.14) | copy-start | bytes 1081348
  63.7 29.5 %copy-start.7 = (bf16[256]{0:T(256)(128)(2,1)S(1)}, bf16[256]{0:T(256)(128)(2,1)}, u32[]{:S(2)}) copy-start(bf16[256]{0:T(256)(128)(2,1)} %param.15) | copy-start | bytes 1540
  63.7 25.2 %all-to-all-start.2 = ((f32[16,24,256]{2,1,0:T(8,128)}), f32[16,24,256]{2,1,0:T(8,128)S(1)}, u32[]{:S(2)}, u32[]{:S(2)}) async-start(f32[16,24,256]{2,1,0:T(8,128)} %fusion.8), calls=%async_computation.2 | async-start | bytes 786432 | tf_op jit(solution)/shard_map/all_to_all | solution.py:23
  74.5 28.7 %copy-start.4 = (bf16[256,704]{0,1:T(8,128)(2,1)S(1)}, bf16[256,704]{0,1:T(8,128)(2,1)}, u32[]{:S(2)}) copy-start(bf16[256,704]{0,1:T(8,128)(2,1)} %param.17) | copy-start | bytes 1081348
  89.7 14.9 %copy-start.5 = (bf16[256,704]{0,1:T(8,128)(2,1)S(1)}, bf16[256,704]{0,1:T(8,128)(2,1)}, u32[]{:S(2)}) copy-start(bf16[256,704]{0,1:T(8,128)(2,1)} %param.16) | copy-start | bytes 1081348
  89.7 13.2 %all-to-all-start.3 = ((bf16[16,24,256]{2,1,0:T(8,128)(2,1)}), bf16[16,24,256]{2,1,0:T(8,128)(2,1)S(1)}, u32[]{:S(2)}, u32[]{:S(2)}) async-start(bf16[16,24,256]{2,1,0:T(8,128)(2,1)} %broadcast_in_dim.9), calls=%async_computation.3 | async-start | bytes 393216 | tf_op jit(solution)/shard_map/all_to_all | solution.py:36
  145.0 14.3 %copy-start.6 = (bf16[704,256]{1,0:T(8,128)(2,1)S(1)}, bf16[704,256]{1,0:T(8,128)(2,1)}, u32[]{:S(2)}) copy-start(bf16[704,256]{1,0:T(8,128)(2,1)} %param.18) | copy-start | bytes 1081348
  160.3 24.2 %copy-start.8 = (bf16[256]{0:T(256)(128)(2,1)S(1)}, bf16[256]{0:T(256)(128)(2,1)}, u32[]{:S(2)}) copy-start(bf16[256]{0:T(256)(128)(2,1)} %param.19) | copy-start | bytes 1540
  160.3 20.1 %all-to-all-start.6 = ((f32[16,24,256]{2,1,0:T(8,128)}), f32[16,24,256]{2,1,0:T(8,128)S(1)}, u32[]{:S(2)}, u32[]{:S(2)}) async-start(f32[16,24,256]{2,1,0:T(8,128)} %fusion.2), calls=%async_computation.6 | async-start | bytes 786432 | tf_op jit(solution)/shard_map/all_to_all | solution.py:23
  181.1 13.0 %all-to-all-start.7 = ((bf16[16,24,256]{2,1,0:T(8,128)(2,1)}), bf16[16,24,256]{2,1,0:T(8,128)(2,1)S(1)}, u32[]{:S(2)}, u32[]{:S(2)}) async-start(bf16[16,24,256]{2,1,0:T(8,128)(2,1)} %broadcast_in_dim.11), calls=%async_computation.7 | async-start | bytes 393216 | tf_op jit(solution)/shard_map/all_to_all | solution.py:36
where the time goes:
time: 212 us; the launch traced here: 209 us
  blocking collectives  114 us (54%)
  waiting for transfers between devices  48.1 us (23%)
  starting transfers between devices  23.3 us (11%)
  matrix products  8.6 us (4%)
  local copies, waits for them, and re-layouts  7.42 us (4%)
  other arithmetic  7.07 us (3%)
    all_to_all x2, blocking collectives, sum_at_owner(): lax.all_to_all(in_blocks(value, dim, length), axis, 0, 0, tiled=True)  72.3 us
    all_to_all x2, waiting for transfers between devices, sum_at_owner(): lax.all_to_all(in_blocks(value, dim, length), axis, 0, 0, tiled=True)  28.9 us
    all_to_all x2, blocking collectives, from_everyone(): lax.all_to_all(jnp.broadcast_to(value[None], (length, *value.shape)), axi...  28.2 us
    all_to_all x2, waiting for transfers between devices, from_everyone(): lax.all_to_all(jnp.broadcast_to(value[None], (length, *value.shape)), axi...  19.2 us
    all_to_all x2, starting transfers between devices, sum_at_owner(): lax.all_to_all(in_blocks(value, dim, length), axis, 0, 0, tiled=True)  16.3 us
    psum x2, blocking collectives, over_axes(): value = lax.psum(value, axis)  13.7 us
    all_to_all x2, starting transfers between devices, from_everyone(): lax.all_to_all(jnp.broadcast_to(value[None], (length, *value.shape)), axi...  6.97 us
    concatenate x4, local copies, waits for them, and re-layouts, sent_together(): both = jnp.concatenate(arrays, axis=along)  5.83 us
  transfers between devices with their start and end apart: 4, of which 4 were waited for; matrix products, arithmetic and copies ran while one was open for 0% of the time, Pallas kernels for 0%

commit v1 on v0

v1 whole, which is shorter than its diff:
```python
import jax
import jax.numpy as jnp
from jax import lax
from jax.sharding import PartitionSpec as P

D = 4096
norm_eps = 1e-06
residual_weight = 0.25
branch_weight = 0.5
bf16 = jnp.bfloat16
f32 = jnp.float32
CHUNK_ROWS = (24,)


def exchange(blocks, axis):
    return lax.all_to_all(blocks, axis, 0, 0, tiled=True)


def to_everyone(value, axis):
    length = lax.axis_size(axis)
    return exchange(jnp.broadcast_to(value[None], (length, *value.shape)), axis)


def in_two(value):
    high = value.astype(bf16)
    return high, (value - high.astype(f32)).astype(bf16)


def gate_up_parts(values, gain, weights, hidden):
    values = values.astype(f32)
    squares = jnp.sum(values * values, axis=1, keepdims=True)
    high, low = in_two(squares)
    normed = (values * gain.astype(f32)).astype(bf16)
    both = jnp.dot(normed, weights, preferred_element_type=f32).astype(bf16)
    lane = lax.broadcasted_iota(jnp.int32, both.shape, 1)
    both = jnp.where(lane == 2 * hidden, high, both)
    return jnp.where(lane == 2 * hidden + 1, low, both)


def hidden_of(blocks, hidden):
    total = jnp.sum(blocks.astype(f32), axis=0)
    squares = total[:, 2 * hidden : 2 * hidden + 1] + total[:, 2 * hidden + 1 : 2 * hidden + 2]
    scale = lax.rsqrt(squares / D + norm_eps)
    gate = total[:, :hidden] * scale
    upper = total[:, hidden : 2 * hidden] * scale
    return (jax.nn.silu(gate) * upper).astype(bf16)


def joined(w_gate, w_up):
    hidden = w_gate.shape[1]
    width = -(-(2 * hidden + 2) // 128) * 128
    return jnp.concatenate(
        [w_gate, w_up, jnp.zeros((w_gate.shape[0], width - 2 * hidden), bf16)], axis=1
    )


def half_step(streams, owned, gain, weights, w_down):
    hidden = w_down.shape[0]
    ra, cb = lax.axis_size("ra"), lax.axis_size("cb")
    parts = [gate_up_parts(s, gain, weights, hidden) for s in streams]
    parts = [exchange(p.reshape(ra, -1, p.shape[1]), "ra") for p in parts]
    hids = [to_everyone(hidden_of(p, hidden), "ra") for p in parts]
    branch = [
        jnp.dot(h.reshape(-1, hidden), w_down, preferred_element_type=f32).astype(bf16) for h in hids
    ]
    branch = [exchange(b.reshape(cb, -1, b.shape[1]), "cb") for b in branch]
    updated = [
        (residual_weight * o.astype(f32) + branch_weight * jnp.sum(b.astype(f32), axis=0)).astype(bf16)
        for o, b in zip(owned, branch)
    ]
    return [to_everyone(u, "cb").reshape(-1, u.shape[1]) for u in updated], updated


def body(
    hidden_states,
    gain_first,
    gate_first,
    up_first,
    down_first,
    gain_second,
    gate_second,
    up_second,
    down_second,
    gain_last,
):
    cb = lax.axis_size("cb")
    me = lax.axis_index("cb")
    streams, owned, start = [], [], 0
    for rows in CHUNK_ROWS:
        stream = hidden_states[start : start + rows * cb]
        streams.append(stream)
        owned.append(lax.dynamic_slice_in_dim(stream, me * rows, rows, 0))
        start += rows * cb
    first, owned = half_step(streams, owned, gain_first, joined(gate_first, up_first), down_first)
    second, _ = half_step(first, owned, gain_second, joined(gate_second, up_second), down_second)
    closed = []
    for s in second:
        values = s.astype(f32)
        squares = jnp.sum(to_everyone(jnp.sum(values * values, axis=1), "ra"), axis=0)
        scale = lax.rsqrt(squares / D + norm_eps)[:, None]
        closed.append((values * scale * gain_last.astype(f32)).astype(bf16))
    return jnp.concatenate(closed, axis=0)


def solution(mesh):
    return jax.shard_map(
        body,
        mesh=mesh,
        in_specs=(
            P(None, "ra"),
            P("ra"),
            P("ra", "cb"),
            P("ra", "cb"),
            P("cb", "ra"),
            P("ra"),
            P("ra", "cb"),
            P("ra", "cb"),
            P("cb", "ra"),
            P("ra"),
        ),
        out_specs=P(None, "ra"),
        check_vma=False,
    )
```

time: 212 us -> 157 us (0.74); the launches traced: 209 us -> 156 us
  waiting for transfers between devices: 48.1 us -> 26.5 us
  blocking collectives: 114 us -> 101 us
  local copies, waits for them, and re-layouts: 7.42 us -> 1.63 us
  starting transfers between devices: 23.3 us -> 18.4 us
  matrix products: 8.6 us -> 3.71 us
  other arithmetic: 7.07 us -> 4.65 us
    all_to_all x4 -> x3, waiting for transfers between devices: 48.1 us -> 26.5 us  [exchange(): return lax.all_to_all(blocks, axis, 0, 0, tiled=True)]
    psum x2 -> x0, blocking collectives: 13.7 us -> none  [over_axes(): value = lax.psum(value, axis)]
    concatenate x4 -> x1, local copies, waits for them, and re-layouts: 5.83 us -> 0.01 us  [joined(): jnp.concatenate([w_gate, w_up, jnp.zeros((w_gate.shape[0], width - 2 * hi...]
    all_to_all x4 -> x3, starting transfers between devices: 23.3 us -> 18.4 us  [exchange(): return lax.all_to_all(blocks, axis, 0, 0, tiled=True)]
    dot_general x6 -> x4, matrix products: 8.6 us -> 3.71 us  [the longest x2 2.4 us: gate_up_parts(): both = jnp.dot(normed, weights, preferred_element_type=f32).astype(bf16)]
    reduce_sum x7 -> x8, other arithmetic: 4.97 us -> 1.79 us  [the longest x2 1.24 us: gate_up_parts(): squares = jnp.sum(values * values, axis=1, keepdims=True)]
    all_to_all x4 -> x6, blocking collectives: 101 us -> 101 us  [exchange(): return lax.all_to_all(blocks, axis, 0, 0, tiled=True)]
  transfers between devices with their start and end apart: 4 -> 3, of which waited for: 4 -> 3; matrix products, arithmetic and copies ran while one was open for 0% -> 0% of each run, Pallas kernels for 0% -> 0%
where the time goes in v1:
time: 157 us; the launch traced here: 156 us
  blocking collectives  101 us (64%)
  waiting for transfers between devices  26.5 us (17%)
  starting transfers between devices  18.4 us (12%)
  other arithmetic  4.65 us (3%)
  matrix products  3.71 us (2%)
  local copies, waits for them, and re-layouts  1.63 us (1%)
    all_to_all x6, blocking collectives, exchange(): return lax.all_to_all(blocks, axis, 0, 0, tiled=True)  101 us
    all_to_all x3, waiting for transfers between devices, exchange(): return lax.all_to_all(blocks, axis, 0, 0, tiled=True)  26.5 us
    all_to_all x3, starting transfers between devices, exchange(): return lax.all_to_all(blocks, axis, 0, 0, tiled=True)  18.4 us
  transfers between devices with their start and end apart: 3, of which 3 were waited for; matrix products, arithmetic and copies ran while one was open for 0% of the time, Pallas kernels for 0%

profile of v1, /device:TPU:1, one launch (start us, length us, event | category | flops | bytes accessed | tf_op | source)
XLA Modules:
  0.0 156.3 jit_solution(1332033411881513366)
XLA Ops:
  0.0 0.0 copy-start
  0.0 1.1 fusion.12
  1.1 0.7 convert_element_type.140
  1.8 1.8 %fusion.3 = bf16[384,1536]{1,0:T(8,128)(2,1)S(1)} fusion(pred[1536]{0:T(1024)(128)(4,1)S(1)} %get-tuple-element.9, pred[1536]{0:T(1024)(128)(4,1)S(1)} %get-tuple-element.10, bf16[256,704]{0,1:T(8,128)(2,1)} %param.13, bf16[256,704]{0,1:T(8,128)(2,1)} %param.12, bf16[384]{0:T(512)(128)(2,1)S(1)} %get-tuple-element.8, ...), kind=kOutput, calls=%fused_computation.5 | convolution fusion | flops 306413568 | bytes 2105856 | tf_op jit(solution)/shard_map/dot_general | solution.py:34
  3.6 24.9 %all_to_all.46 = bf16[16,24,1536]{2,1,0:T(8,128)(2,1)S(1)} all-to-all(bf16[16,24,1536]{2,1,0:T(8,128)(2,1)S(1)} %bitcast.24), channel_id=1, replica_groups=mesh['ra'=16,'cb'=16] {'ra'}, dimensions={0} | all-to-all | bytes 2359296 | tf_op jit(solution)/shard_map/all_to_all | solution.py:16
  28.5 0.2 convert_reduce_fusion.1
  28.6 0.2 fusion.32
  28.8 0.1 fusion.24
  29.0 13.5 %all_to_all.47 = bf16[16,24,704]{2,1,0:T(8,128)(2,1)S(1)} all-to-all(bf16[16,24,704]{2,1,0:T(8,128)(2,1)S(1)} %broadcast_in_dim.63), channel_id=1, replica_groups=mesh['ra'=16,'cb'=16] {'ra'}, dimensions={0} | all-to-all | bytes 1081344 | tf_op jit(solution)/shard_map/all_to_all | solution.py:16
  42.5 0.0 copy-done
  42.5 0.0 copy-start.4
  42.5 1.0 convolution_convert_fusion.3
  43.5 0.0 copy-start.2
  43.5 0.0 copy-start.3
  43.5 11.4 %all-to-all-start.2 = ((bf16[16,24,256]{2,1,0:T(8,128)(2,1)}), bf16[16,24,256]{2,1,0:T(8,128)(2,1)S(1)}, u32[]{:S(2)}, u32[]{:S(2)}) async-start(bf16[16,24,256]{2,1,0:T(8,128)(2,1)} %bitcast.2), calls=%async_computation.2 | async-start | bytes 393216 | tf_op jit(solution)/shard_map/all_to_all | solution.py:16
  54.9 10.2 %all-to-all-done.2 = bf16[16,24,256]{2,1,0:T(8,128)(2,1)S(1)} async-done(((bf16[16,24,256]{2,1,0:T(8,128)(2,1)}), bf16[16,24,256]{2,1,0:T(8,128)(2,1)S(1)}, u32[]{:S(2)}, u32[]{:S(2)}) %all-to-all-start.2) | async-done | bytes 196640 | tf_op jit(solution)/shard_map/all_to_all | solution.py:16
  65.2 0.7 add_convert_fusion.1
  65.9 0.7 broadcast_in_dim.64
  66.6 3.4 %all-to-all-start.3 = ((bf16[16,24,256]{2,1,0:T(8,128)(2,1)}), bf16[16,24,256]{2,1,0:T(8,128)(2,1)S(1)}, u32[]{:S(2)}, u32[]{:S(2)}) async-start(bf16[16,24,256]{2,1,0:T(8,128)(2,1)} %broadcast_in_dim.64), calls=%async_computation.3 | async-start | bytes 393216 | tf_op jit(solution)/shard_map/all_to_all | solution.py:16
  70.0 0.0 copy-done.4
  70.0 9.8 %all-to-all-done.3 = bf16[16,24,256]{2,1,0:T(8,128)(2,1)S(1)} async-done(((bf16[16,24,256]{2,1,0:T(8,128)(2,1)}), bf16[16,24,256]{2,1,0:T(8,128)(2,1)S(1)}, u32[]{:S(2)}, u32[]{:S(2)}) %all-to-all-start.3) | async-done | bytes 196640 | tf_op jit(solution)/shard_map/all_to_all | solution.py:16
  79.8 0.1 multiply_reduce_fusion.1
  79.9 0.1 reduce_sum.78
  80.1 0.0 copy-done.2
  80.1 0.0 copy-done.3
  80.1 0.6 fusion.2
  80.7 21.2 %all_to_all.48 = bf16[16,24,1536]{2,1,0:T(8,128)(2,1)S(1)} all-to-all(bf16[16,24,1536]{2,1,0:T(8,128)(2,1)S(1)} %bitcast.23), channel_id=1, replica_groups=mesh['ra'=16,'cb'=16] {'ra'}, dimensions={0} | all-to-all | bytes 2359296 | tf_op jit(solution)/shard_map/all_to_all | solution.py:16
  101.9 0.2 convert_reduce_fusion
  102.0 0.0 copy-start.1
  102.1 0.2 fusion.28
  102.2 0.1 fusion.22
  102.4 14.1 %all_to_all.49 = bf16[16,24,704]{2,1,0:T(8,128)(2,1)S(1)} all-to-all(bf16[16,24,704]{2,1,0:T(8,128)(2,1)S(1)} %broadcast_in_dim.67), channel_id=1, replica_groups=mesh['ra'=16,'cb'=16] {'ra'}, dimensions={0} | all-to-all | bytes 1081344 | tf_op jit(solution)/shard_map/all_to_all | solution.py:16
  116.5 0.0 copy-done.1
  116.5 0.0 copy-start.5
  116.5 0.3 convolution_convert_fusion.2
  116.9 14.7 %all_to_all.50 = bf16[16,24,256]{2,1,0:T(8,128)(2,1)S(1)} all-to-all(bf16[16,24,256]{2,1,0:T(8,128)(2,1)S(1)} %bitcast.25), channel_id=1, replica_groups=mesh['ra'=16,'cb'=16] {'cb'}, dimensions={0} | all-to-all | bytes 393216 | tf_op jit(solution)/shard_map/all_to_all | solution.py:16
  131.6 13.0 %all_to_all.51 = bf16[16,24,256]{2,1,0:T(8,128)(2,1)S(1)} all-to-all(bf16[16,24,256]{2,1,0:T(8,128)(2,1)S(1)} %broadcast_in_dim.68), channel_id=1, replica_groups=mesh['ra'=16,'cb'=16] {'cb'}, dimensions={0} | all-to-all | bytes 393216 | tf_op jit(solution)/shard_map/all_to_all | solution.py:16
  144.6 0.1 multiply_reduce_fusion
  144.7 0.1 broadcast_in_dim.69
  144.8 0.6 broadcast_in_dim.70
  145.4 3.5 %all-to-all-start.8 = ((f32[16,1,384]{2,1,0:T(1,128)}), f32[16,1,384]{2,1,0:T(1,128)S(1)}, u32[]{:S(2)}, u32[]{:S(2)}) async-start(f32[16,1,384]{2,1,0:T(1,128)} %broadcast_in_dim.70), calls=%async_computation.8 | async-start | bytes 49152 | tf_op jit(solution)/shard_map/all_to_all | solution.py:16
  148.9 0.0 copy-done.5
  148.9 6.5 %all-to-all-done.8 = f32[16,1,384]{2,1,0:T(1,128)S(1)} async-done(((f32[16,1,384]{2,1,0:T(1,128)}), f32[16,1,384]{2,1,0:T(1,128)S(1)}, u32[]{:S(2)}, u32[]{:S(2)}) %all-to-all-start.8) | async-done | bytes 24608 | tf_op jit(solution)/shard_map/all_to_all | solution.py:16
  155.5 0.8 fusion.17
  (16 shorter events, 0.3 us)
Async XLA Ops:
  0.0 42.5 %copy-start = (bf16[704,256]{1,0:T(8,128)(2,1)S(1)}, bf16[704,256]{1,0:T(8,128)(2,1)}, u32[]{:S(2)}) copy-start(bf16[704,256]{1,0:T(8,128)(2,1)} %param.14) | copy-start | bytes 1081348
  42.5 27.5 %copy-start.4 = (bf16[256]{0:T(256)(128)(2,1)S(1)}, bf16[256]{0:T(256)(128)(2,1)}, u32[]{:S(2)}) copy-start(bf16[256]{0:T(256)(128)(2,1)} %param.15) | copy-start | bytes 1540
  43.5 36.6 %copy-start.2 = (bf16[256,704]{0,1:T(8,128)(2,1)S(1)}, bf16[256,704]{0,1:T(8,128)(2,1)}, u32[]{:S(2)}) copy-start(bf16[256,704]{0,1:T(8,128)(2,1)} %param.17) | copy-start | bytes 1081348
  43.5 36.6 %copy-start.3 = (bf16[256,704]{0,1:T(8,128)(2,1)S(1)}, bf16[256,704]{0,1:T(8,128)(2,1)}, u32[]{:S(2)}) copy-start(bf16[256,704]{0,1:T(8,128)(2,1)} %param.16) | copy-start | bytes 1081348
  43.5 21.6 %all-to-all-start.2 = ((bf16[16,24,256]{2,1,0:T(8,128)(2,1)}), bf16[16,24,256]{2,1,0:T(8,128)(2,1)S(1)}, u32[]{:S(2)}, u32[]{:S(2)}) async-start(bf16[16,24,256]{2,1,0:T(8,128)(2,1)} %bitcast.2), calls=%async_computation.2 | async-start | bytes 393216 | tf_op jit(solution)/shard_map/all_to_all | solution.py:16
  66.6 13.2 %all-to-all-start.3 = ((bf16[16,24,256]{2,1,0:T(8,128)(2,1)}), bf16[16,24,256]{2,1,0:T(8,128)(2,1)S(1)}, u32[]{:S(2)}, u32[]{:S(2)}) async-start(bf16[16,24,256]{2,1,0:T(8,128)(2,1)} %broadcast_in_dim.64), calls=%async_computation.3 | async-start | bytes 393216 | tf_op jit(solution)/shard_map/all_to_all | solution.py:16
  102.0 14.5 %copy-start.1 = (bf16[704,256]{1,0:T(8,128)(2,1)S(1)}, bf16[704,256]{1,0:T(8,128)(2,1)}, u32[]{:S(2)}) copy-start(bf16[704,256]{1,0:T(8,128)(2,1)} %param.18) | copy-start | bytes 1081348
  116.5 32.4 %copy-start.5 = (bf16[256]{0:T(256)(128)(2,1)S(1)}, bf16[256]{0:T(256)(128)(2,1)}, u32[]{:S(2)}) copy-start(bf16[256]{0:T(256)(128)(2,1)} %param.19) | copy-start | bytes 1540
  145.4 10.0 %all-to-all-start.8 = ((f32[16,1,384]{2,1,0:T(1,128)}), f32[16,1,384]{2,1,0:T(1,128)S(1)}, u32[]{:S(2)}, u32[]{:S(2)}) async-start(f32[16,1,384]{2,1,0:T(1,128)} %broadcast_in_dim.70), calls=%async_computation.8 | async-start | bytes 49152 | tf_op jit(solution)/shard_map/all_to_all | solution.py:16

commit v2 on v1

v2 whole, which is shorter than its diff:
```python
import functools

import jax
import jax.numpy as jnp
from jax import lax
from jax.experimental import pallas as pl
from jax.experimental.pallas import tpu as pltpu
from jax.sharding import Mesh
from jax.sharding import PartitionSpec as P

norm_eps = 1e-06
residual_weight = 0.25
branch_weight = 0.5
bf16 = jnp.bfloat16
f32 = jnp.float32
TILE = 8
HALF = TILE // 2


def exchange(blocks, axis):
    return lax.all_to_all(blocks, axis, 0, 0, tiled=True)


def partner(value):
    return lax.ppermute(value, "c", [(0, 1), (1, 0)])


def rolled(value):
    return pltpu.roll(value, HALF, value.ndim - 2)


def first_half(shape):
    return lax.broadcasted_iota(jnp.int32, shape, len(shape) - 2) < HALF


def gate_up_kernel(group, hidden, x, gain, *refs):
    weights, out, padded = refs[:4], refs[4], refs[5]
    wide = out.shape[2]
    values = x[...].astype(f32)
    squares = jnp.sum(values * values, axis=1, keepdims=True)
    high = squares.astype(bf16).astype(f32)
    low = squares - high
    normed = (values * gain[...].astype(f32)).astype(bf16)
    lane = lax.broadcasted_iota(jnp.int32, (values.shape[0], wide), 1)
    padded[hidden:] = jnp.zeros((wide - hidden, padded.shape[1]), bf16)
    sums = []
    for weight in weights:
        padded[:hidden] = weight[...]
        sums.append(lax.dot_general(normed, padded[...], (((1,), (1,)), ((), ())), preferred_element_type=f32))
    sums[0] = jnp.where(lane == hidden, high, jnp.where(lane == hidden + 1, low, sums[0]))
    whole = group * TILE
    for k in range(2):
        gate, up = sums[2 * k], sums[2 * k + 1]
        at = 3 * TILE * k
        out[:, at : at + TILE] = gate[:whole].reshape(group, TILE, wide).astype(bf16)
        out[:, at + TILE : at + 2 * TILE] = up[:whole].reshape(group, TILE, wide).astype(bf16)
        gate = gate[whole:].reshape(group // 2, TILE, wide)
        up = up[whole:].reshape(group // 2, TILE, wide)
        first = first_half(gate.shape)
        even = jnp.where(first, gate, rolled(up))
        odd = jnp.where(first, rolled(gate), up)
        both = jnp.stack([even, odd], axis=1).reshape(group, TILE, wide)
        out[:, at + 2 * TILE : at + 3 * TILE] = both.astype(bf16)


def hidden_kernel(group, hidden, features, parts, out):
    total = parts[0].astype(f32)
    for k in range(1, group):
        total = total + parts[k].astype(f32)

    def gated(gate, up, scale):
        gate = gate * scale
        return gate * jax.nn.sigmoid(gate) * (up * scale)

    def scale_of(rows):
        squares = rows[:, hidden : hidden + 1] + rows[:, hidden + 1 : hidden + 2]
        return lax.rsqrt(squares / features + norm_eps)

    scale = scale_of(total[:TILE])
    mixed_scale = scale_of(total[2 * TILE : 3 * TILE])
    tiles, mixed = [], []
    for k in range(2):
        at = 3 * TILE * k
        tiles.append(gated(total[at : at + TILE], total[at + TILE : at + 2 * TILE], scale))
        both = total[at + 2 * TILE : at + 3 * TILE]
        mixed.append(gated(both, rolled(both), mixed_scale))
    tiles.append(jnp.where(first_half(mixed[0].shape), mixed[0], rolled(mixed[1])))
    rows = jnp.concatenate(tiles, axis=0)[:, :hidden].astype(bf16)
    for k in range(group):
        out[k] = rows


def down_kernel(group, hids, own, other, out):
    hidden, width = own.shape
    tiles = [
        hids[:, TILE * k : TILE * (k + 1)].astype(f32).reshape(group * TILE, hidden).astype(bf16) for k in range(3)
    ]
    dot = functools.partial(jnp.dot, preferred_element_type=f32)
    whole = dot(tiles[0], own[...]) + dot(tiles[1], other[...])
    mixed = dot(tiles[2], own[...]).reshape(group, TILE, width)
    mixed = mixed + rolled(dot(tiles[2], other[...]).reshape(group, TILE, width))
    mixed = mixed.reshape(group // 2, 2, TILE, width)
    even, odd = mixed[:, 0], mixed[:, 1]
    rest = jnp.where(first_half(even.shape), even, rolled(odd)).reshape(group // 2 * TILE, width)
    rows = jnp.concatenate([whole, rest], axis=0)
    out[...] = rows.reshape(out.shape).astype(bf16)


def update_kernel(group, parts, start, out, kept):
    total = parts[0].astype(f32)
    for k in range(1, group):
        total = total + parts[k].astype(f32)
    rows = (residual_weight * start[...].astype(f32) + branch_weight * total).astype(bf16)
    kept[...] = rows
    for k in range(group):
        out[k] = rows


def kernel_call(kernel, outs, scratch=()):
    inside = pl.BlockSpec(memory_space=pltpu.VMEM)
    many = isinstance(outs, list)

    def call(*args):
        return pl.pallas_call(
            kernel,
            out_shape=outs,
            in_specs=[inside] * len(args),
            out_specs=[inside] * len(outs) if many else inside,
            scratch_shapes=scratch,
            compiler_params=pltpu.CompilerParams(vmem_limit_bytes=12 * 2**20),
        )(*args)

    return call


def half_step(stream, start, gain, gates, ups, downs, features):
    ra, z = lax.axis_size("ra"), lax.axis_size("z")
    tokens, width = stream.shape
    hidden = gates[0].shape[0]
    wide = -(-(hidden + 2) // 128) * 128
    parts = kernel_call(
        functools.partial(gate_up_kernel, ra, hidden),
        jax.ShapeDtypeStruct((ra, 6 * TILE, wide), bf16),
        [pltpu.VMEM((wide, width), bf16)],
    )(stream, gain[None], gates[0], ups[0], gates[1], ups[1])
    parts = exchange(parts, "ra")
    hids = kernel_call(
        functools.partial(hidden_kernel, ra, hidden, features),
        jax.ShapeDtypeStruct((ra, 3 * TILE, hidden), bf16),
    )(parts)
    hids = exchange(hids, "ra")
    branch = kernel_call(
        functools.partial(down_kernel, ra),
        jax.ShapeDtypeStruct((z, tokens // z, width), bf16),
    )(hids, downs[0], downs[1])
    branch = exchange(branch, "z")
    updated, kept = kernel_call(
        functools.partial(update_kernel, z),
        [
            jax.ShapeDtypeStruct((z, tokens // z, width), bf16),
            jax.ShapeDtypeStruct((tokens // z, width), bf16),
        ],
    )(branch, start)
    return exchange(updated, "z").reshape(tokens, width), kept


def body(
    hidden_states,
    gain_first,
    gate_first,
    up_first,
    down_first,
    gain_second,
    gate_second,
    up_second,
    down_second,
    gain_last,
):
    features = hidden_states.shape[1] * lax.axis_size("ra")
    tokens = hidden_states.shape[0] // lax.axis_size("c")
    core = lax.axis_index("c")
    rows = tokens // lax.axis_size("z")
    stream = lax.dynamic_slice_in_dim(hidden_states, core * tokens, tokens, 0)
    start = lax.dynamic_slice_in_dim(hidden_states, core * tokens + lax.axis_index("z") * rows, rows, 0)
    pairs = [
        (w, partner(w)) for w in (gate_first.T, up_first.T, down_first, gate_second.T, up_second.T, down_second)
    ]
    first, start = half_step(stream, start, gain_first, *pairs[:3], features)
    second, _ = half_step(first, start, gain_second, *pairs[3:], features)
    other = partner(second)
    both = jnp.where(core == 0, jnp.concatenate([second, other], 0), jnp.concatenate([other, second], 0))
    values = both.astype(f32)
    squares = jnp.sum(values * values, axis=1)
    length = lax.axis_size("ra")
    squares = jnp.sum(exchange(jnp.broadcast_to(squares[None], (length, squares.shape[0])), "ra"), axis=0)
    scale = lax.rsqrt(squares / features + norm_eps)[:, None]
    return (values * scale * gain_last.astype(f32)).astype(bf16)


def solution(mesh):
    split = Mesh(mesh.devices.reshape(mesh.shape["ra"], -1, 2), ("ra", "z", "c"))
    cb = ("z", "c")
    return jax.shard_map(
        body,
        mesh=split,
        in_specs=(
            P(None, "ra"),
            P("ra"),
            P("ra", cb),
            P("ra", cb),
            P(cb, "ra"),
            P("ra"),
            P("ra", cb),
            P("ra", cb),
            P(cb, "ra"),
            P("ra"),
        ),
        out_specs=P(None, "ra"),
        check_vma=False,
    )
```

time: 157 us -> 150 us (0.955)
  blocking collectives: 101 us -> 60.1 us
  starting transfers between devices: 18.4 us -> 42.2 us
  waiting for transfers between devices: 26.5 us -> 36.1 us
  Pallas kernels: 0 us -> 6.26 us
  matrix products: 3.71 us -> 0 us
  other arithmetic: 4.65 us -> 1.01 us
  local copies, waits for them, and re-layouts: 1.63 us -> 3.3 us
    all_to_all x6 -> x4, blocking collectives: 101 us -> 60.1 us  [exchange(): return lax.all_to_all(blocks, axis, 0, 0, tiled=True)]
    ppermute x0 -> x7, starting transfers between devices: none -> 20 us  [partner(): return lax.ppermute(value, 'c', [(0, 1), (1, 0)])]
    pallas_call x0 -> x8, Pallas kernels: none -> 6.26 us  [call(): pl.pallas_call(kernel, out_shape=outs, in_specs=[inside] * len(args), out...]
    all_to_all x3 -> x5, waiting for transfers between devices: 26.5 us -> 31.7 us  [exchange(): return lax.all_to_all(blocks, axis, 0, 0, tiled=True)]
    ppermute x0 -> x7, waiting for transfers between devices: none -> 4.39 us  [partner(): return lax.ppermute(value, 'c', [(0, 1), (1, 0)])]
    all_to_all x3 -> x5, starting transfers between devices: 18.4 us -> 22.2 us  [exchange(): return lax.all_to_all(blocks, axis, 0, 0, tiled=True)]
    dot_general x4 -> x0, matrix products: 3.71 us -> none  [the longest x2 2.4 us: gate_up_parts(): both = jnp.dot(normed, weights, preferred_element_type=f32).astype(bf16)]
    unnamed x12 -> x18, local copies, waits for them, and re-layouts: 0.02 us -> 2 us
  transfers between devices with their start and end apart: 3 -> 12, of which waited for: 3 -> 10; matrix products, arithmetic and copies ran while one was open for 0% -> 0% of each run, Pallas kernels for 0% -> 1%
where the time goes in v2:
time: 150 us; the launch traced here: 149 us
  blocking collectives  60.1 us (40%)
  starting transfers between devices  42.2 us (28%)
  waiting for transfers between devices  36.1 us (24%)
  Pallas kernels  6.26 us (4%)
  local copies, waits for them, and re-layouts  3.3 us (2%)
    all_to_all x4, blocking collectives, exchange(): return lax.all_to_all(blocks, axis, 0, 0, tiled=True)  60.1 us
    all_to_all x5, waiting for transfers between devices, exchange(): return lax.all_to_all(blocks, axis, 0, 0, tiled=True)  31.7 us
    all_to_all x5, starting transfers between devices, exchange(): return lax.all_to_all(blocks, axis, 0, 0, tiled=True)  22.2 us
    ppermute x7, starting transfers between devices, partner(): return lax.ppermute(value, 'c', [(0, 1), (1, 0)])  20 us
    pallas_call x8, Pallas kernels, call(): pl.pallas_call(kernel, out_shape=outs, in_specs=[inside] * len(args), out...  6.26 us
    ppermute x7, waiting for transfers between devices, partner(): return lax.ppermute(value, 'c', [(0, 1), (1, 0)])  4.39 us
  transfers between devices with their start and end apart: 12, of which 10 were waited for; matrix products, arithmetic and copies ran while one was open for 0% of the time, Pallas kernels for 1%

profile of v2, /device:TPU:1, one launch (start us, length us, event | category | flops | bytes accessed | tf_op | source)
XLA Modules:
  0.0 149.1 jit_solution(8440726469585224674)
XLA Ops:
  0.0 0.0 copy-start
  0.0 3.2 %collective-permute-start = (bf16[704,256]{1,0:T(8,128)(2,1)}, bf16[704,256]{1,0:T(8,128)(2,1)S(1)}, u32[]{:S(2)}, u32[]{:S(2)}) collective-permute-start(bf16[704,256]{1,0:T(8,128)(2,1)} %bitcast.7), channel_id=1, source_target_pairs={{0,1},{1,0},{2,3},{3,2},{4,5},{5,4},{6,7},{7,6},{8,9},{9,8},{10,11... | collective-permute-start | bytes 1081352 | tf_op jit(solution)/shard_map/ppermute | solution.py:25
  3.2 0.0 collective-permute-start.1
  3.2 0.7 broadcast_in_dim.6.gain
  3.9 0.8 collective-permute-done.refs_2_
  4.7 0.5 collective-permute-done.1.refs_3_
  5.2 1.0 copy-done.1
  6.2 1.0 copy-done.2
  7.2 0.7 shard_map.100
  7.9 22.9 %all_to_all.46.parts = bf16[16,48,768]{2,1,0:T(8,128)(2,1)S(1)} all-to-all(bf16[16,48,768]{2,1,0:T(8,128)(2,1)S(1)} %shard_map.100), channel_id=1, replica_groups=mesh['ra'=16,'z'=8,'c'=2] {'ra'}, dimensions={0} | all-to-all | bytes 2359296 | tf_op jit(solution)/shard_map/all_to_all | solution.py:21
  30.8 1.1 shard_map.101
  31.9 3.6 %all-to-all-start.1 = ((bf16[16,24,704]{2,1,0:T(8,128)(2,1)}), bf16[16,24,704]{2,1,0:T(8,128)(2,1)S(1)}, u32[]{:S(2)}, u32[]{:S(2)}) async-start(bf16[16,24,704]{2,1,0:T(8,128)(2,1)} %shard_map.101), calls=%async_computation.1 | async-start | bytes 1179648 | tf_op jit(solution)/shard_map/all_to_all | solution.py:21
  35.5 0.0 copy-done.5
  35.5 0.0 copy-start.7
  35.5 1.6 %collective-permute-start.2 = (bf16[704,256]{1,0:T(8,128)(2,1)S(1)}, bf16[704,256]{1,0:T(8,128)(2,1)S(1)}, u32[]{:S(2)}, u32[]{:S(2)}) collective-permute-start(bf16[704,256]{1,0:T(8,128)(2,1)S(1)} %copy-done.5), channel_id=1, source_target_pairs={{0,1},{1,0},{2,3},{3,2},{4,5},{5,4},{6,7},{7,6},{8,9},{9,8},{10,11... | collective-permute-start | bytes 1081352 | tf_op jit(solution)/shard_map/ppermute | solution.py:25
  37.1 0.1 collective-permute-start.3
  37.2 0.0 copy-done.4
  37.2 0.4 collective-permute-start.4
  37.6 0.8 collective-permute-done.2.other
  38.4 8.0 %all-to-all-done.1.hids = bf16[16,24,704]{2,1,0:T(8,128)(2,1)S(1)} async-done(((bf16[16,24,704]{2,1,0:T(8,128)(2,1)}), bf16[16,24,704]{2,1,0:T(8,128)(2,1)S(1)}, u32[]{:S(2)}, u32[]{:S(2)}) %all-to-all-start.1) | async-done | bytes 540704 | tf_op jit(solution)/shard_map/all_to_all | solution.py:21
  46.4 1.0 shard_map.102
  47.4 8.2 %all-to-all-start.2 = ((bf16[8,24,256]{2,1,0:T(8,128)(2,1)}), bf16[8,24,256]{2,1,0:T(8,128)(2,1)S(1)}, u32[]{:S(2)}, u32[]{:S(2)}) async-start(bf16[8,24,256]{2,1,0:T(8,128)(2,1)} %shard_map.102), calls=%async_computation.2 | async-start | bytes 196608 | tf_op jit(solution)/shard_map/all_to_all | solution.py:21
  55.6 7.6 %all-to-all-done.2.parts = bf16[8,24,256]{2,1,0:T(8,128)(2,1)S(1)} async-done(((bf16[8,24,256]{2,1,0:T(8,128)(2,1)}), bf16[8,24,256]{2,1,0:T(8,128)(2,1)S(1)}, u32[]{:S(2)}, u32[]{:S(2)}) %all-to-all-start.2) | async-done | bytes 98336 | tf_op jit(solution)/shard_map/all_to_all | solution.py:21
  63.1 0.7 shard_map.103
  63.8 3.4 %all-to-all-start.3 = ((bf16[8,24,256]{2,1,0:T(8,128)(2,1)}), bf16[8,24,256]{2,1,0:T(8,128)(2,1)S(1)}, u32[]{:S(2)}, u32[]{:S(2)}) async-start(bf16[8,24,256]{2,1,0:T(8,128)(2,1)} %get-tuple-element.8), calls=%async_computation.3 | async-start | bytes 196608 | tf_op jit(solution)/shard_map/all_to_all | solution.py:21
  67.2 0.0 collective-permute-done.3.refs_2_
  67.2 0.0 collective-permute-done.4.refs_3_
  67.2 7.4 %all-to-all-done.3 = bf16[8,24,256]{2,1,0:T(8,128)(2,1)S(1)} async-done(((bf16[8,24,256]{2,1,0:T(8,128)(2,1)}), bf16[8,24,256]{2,1,0:T(8,128)(2,1)S(1)}, u32[]{:S(2)}, u32[]{:S(2)}) %all-to-all-start.3) | async-done | bytes 98336 | tf_op jit(solution)/shard_map/all_to_all | solution.py:21
  74.7 0.7 shard_map.104
  75.3 17.3 %all_to_all.47.parts = bf16[16,48,768]{2,1,0:T(8,128)(2,1)S(1)} all-to-all(bf16[16,48,768]{2,1,0:T(8,128)(2,1)S(1)} %shard_map.104), channel_id=1, replica_groups=mesh['ra'=16,'z'=8,'c'=2] {'ra'}, dimensions={0} | all-to-all | bytes 2359296 | tf_op jit(solution)/shard_map/all_to_all | solution.py:21
  92.6 1.1 shard_map.105
  93.7 3.6 %all-to-all-start.5 = ((bf16[16,24,704]{2,1,0:T(8,128)(2,1)}), bf16[16,24,704]{2,1,0:T(8,128)(2,1)S(1)}, u32[]{:S(2)}, u32[]{:S(2)}) async-start(bf16[16,24,704]{2,1,0:T(8,128)(2,1)} %shard_map.105), calls=%async_computation.5 | async-start | bytes 1179648 | tf_op jit(solution)/shard_map/all_to_all | solution.py:21
  97.3 0.0 copy-done.6
  97.3 0.0 copy-start.8
  97.3 5.6 %collective-permute-start.5 = (bf16[704,256]{1,0:T(8,128)(2,1)S(1)}, bf16[704,256]{1,0:T(8,128)(2,1)S(1)}, u32[]{:S(2)}, u32[]{:S(2)}) collective-permute-start(bf16[704,256]{1,0:T(8,128)(2,1)S(1)} %copy-done.6), channel_id=1, source_target_pairs={{0,1},{1,0},{2,3},{3,2},{4,5},{5,4},{6,7},{7,6},{8,9},{9,8},{10,11... | collective-permute-start | bytes 1081352 | tf_op jit(solution)/shard_map/ppermute | solution.py:25
  102.9 1.3 collective-permute-done.5.other
  104.3 2.4 %all-to-all-done.5.hids = bf16[16,24,704]{2,1,0:T(8,128)(2,1)S(1)} async-done(((bf16[16,24,704]{2,1,0:T(8,128)(2,1)}), bf16[16,24,704]{2,1,0:T(8,128)(2,1)S(1)}, u32[]{:S(2)}, u32[]{:S(2)}) %all-to-all-start.5) | async-done | bytes 540704 | tf_op jit(solution)/shard_map/all_to_all | solution.py:21
  106.6 0.4 shard_map.106
  107.0 10.0 %all_to_all.48.parts = bf16[8,24,256]{2,1,0:T(8,128)(2,1)S(1)} all-to-all(bf16[8,24,256]{2,1,0:T(8,128)(2,1)S(1)} %shard_map.106), channel_id=1, replica_groups=mesh['ra'=16,'z'=8,'c'=2] {'z'}, dimensions={0} | all-to-all | bytes 196608 | tf_op jit(solution)/shard_map/all_to_all | solution.py:21
  117.0 0.6 shard_map.107
  117.6 9.9 %all_to_all.49 = bf16[8,24,256]{2,1,0:T(8,128)(2,1)S(1)} all-to-all(bf16[8,24,256]{2,1,0:T(8,128)(2,1)S(1)} %get-tuple-element.10), channel_id=1, replica_groups=mesh['ra'=16,'z'=8,'c'=2] {'z'}, dimensions={0} | all-to-all | bytes 196608 | tf_op jit(solution)/shard_map/all_to_all | solution.py:21
  127.5 9.1 %collective-permute-start.6 = (bf16[192,256]{1,0:T(8,128)(2,1)S(1)}, bf16[192,256]{1,0:T(8,128)(2,1)S(1)}, u32[]{:S(2)}, u32[]{:S(2)}) collective-permute-start(bf16[192,256]{1,0:T(8,128)(2,1)S(1)} %bitcast.15), channel_id=1, source_target_pairs={{0,1},{1,0},{2,3},{3,2},{4,5},{5,4},{6,7},{7,6},{8,9},{9,8},{10,11... | collective-permute-start | bytes 294920 | tf_op jit(solution)/shard_map/ppermute | solution.py:25
  136.6 0.9 collective-permute-done.6
  137.6 0.1 fusion
  137.7 0.6 broadcast_in_dim.16
  138.3 3.5 %all-to-all-start.8 = ((f32[16,1,384]{2,1,0:T(1,128)}), f32[16,1,384]{2,1,0:T(1,128)S(1)}, u32[]{:S(2)}, u32[]{:S(2)}) async-start(f32[16,1,384]{2,1,0:T(1,128)} %broadcast_in_dim.16), calls=%async_computation.8 | async-start | bytes 49152 | tf_op jit(solution)/shard_map/all_to_all | solution.py:21
  141.9 6.4 %all-to-all-done.8 = f32[16,1,384]{2,1,0:T(1,128)S(1)} async-done(((f32[16,1,384]{2,1,0:T(1,128)}), f32[16,1,384]{2,1,0:T(1,128)S(1)}, u32[]{:S(2)}, u32[]{:S(2)}) %all-to-all-start.8) | async-done | bytes 24608 | tf_op jit(solution)/shard_map/all_to_all | solution.py:21
  148.3 0.8 fusion.2
  (16 shorter events, 0.1 us)
Async XLA Ops:
  0.0 3.9 %copy-start = (bf16[384,256]{1,0:T(8,128)(2,1)S(1)}, bf16[384,256]{1,0:T(8,128)(2,1)}, u32[]{:S(2)}) copy-start(bf16[384,256]{1,0:T(8,128)(2,1)} %param.10) | copy-start | bytes 589828
  0.0 4.7 %collective-permute-start = (bf16[704,256]{1,0:T(8,128)(2,1)}, bf16[704,256]{1,0:T(8,128)(2,1)S(1)}, u32[]{:S(2)}, u32[]{:S(2)}) collective-permute-start(bf16[704,256]{1,0:T(8,128)(2,1)} %bitcast.7), channel_id=1, source_target_pairs={{0,1},{1,0},{2,3},{3,2},{4,5},{5,4},{6,7},{7,6},{8,9},{9,8},{10,11... | collective-permute-start | bytes 1081352 | tf_op jit(solution)/shard_map/ppermute | solution.py:25
  3.2 2.0 %collective-permute-start.1 = (bf16[704,256]{1,0:T(8,128)(2,1)}, bf16[704,256]{1,0:T(8,128)(2,1)S(1)}, u32[]{:S(2)}, u32[]{:S(2)}) collective-permute-start(bf16[704,256]{1,0:T(8,128)(2,1)} %bitcast.9), channel_id=1, source_target_pairs={{0,1},{1,0},{2,3},{3,2},{4,5},{5,4},{6,7},{7,6},{8,9},{9,8},{10,11... | collective-permute-start | bytes 1081352 | tf_op jit(solution)/shard_map/ppermute | solution.py:25
  5.2 1.0 copy-start.1
  6.2 1.0 copy-start.2
  30.8 4.7 %copy-start.5 = (bf16[704,256]{1,0:T(8,128)(2,1)S(1)}, bf16[704,256]{1,0:T(8,128)(2,1)}, u32[]{:S(2)}) copy-start(bf16[704,256]{1,0:T(8,128)(2,1)} %own.2) | copy-start | bytes 1081348
  30.8 6.3 %copy-start.3 = (bf16[256,704]{0,1:T(8,128)(2,1)S(1)}, bf16[256,704]{0,1:T(8,128)(2,1)}, u32[]{:S(2)}) copy-start(bf16[256,704]{0,1:T(8,128)(2,1)} %param.16) | copy-start | bytes 1081348
  30.8 6.4 %copy-start.4 = (bf16[256,704]{0,1:T(8,128)(2,1)S(1)}, bf16[256,704]{0,1:T(8,128)(2,1)}, u32[]{:S(2)}) copy-start(bf16[256,704]{0,1:T(8,128)(2,1)} %param.17) | copy-start | bytes 1081348
  31.9 14.5 %all-to-all-start.1 = ((bf16[16,24,704]{2,1,0:T(8,128)(2,1)}), bf16[16,24,704]{2,1,0:T(8,128)(2,1)S(1)}, u32[]{:S(2)}, u32[]{:S(2)}) async-start(bf16[16,24,704]{2,1,0:T(8,128)(2,1)} %shard_map.101), calls=%async_computation.1 | async-start | bytes 1179648 | tf_op jit(solution)/shard_map/all_to_all | solution.py:21
  35.5 31.7 %copy-start.7 = (bf16[256]{0:T(256)(128)(2,1)S(1)}, bf16[256]{0:T(256)(128)(2,1)}, u32[]{:S(2)}) copy-start(bf16[256]{0:T(256)(128)(2,1)} %param.15) | copy-start | bytes 1540
  35.5 2.9 %collective-permute-start.2 = (bf16[704,256]{1,0:T(8,128)(2,1)S(1)}, bf16[704,256]{1,0:T(8,128)(2,1)S(1)}, u32[]{:S(2)}, u32[]{:S(2)}) collective-permute-start(bf16[704,256]{1,0:T(8,128)(2,1)S(1)} %copy-done.5), channel_id=1, source_target_pairs={{0,1},{1,0},{2,3},{3,2},{4,5},{5,4},{6,7},{7,6},{8,9},{9,8},{10,11... | collective-permute-start | bytes 1081352 | tf_op jit(solution)/shard_map/ppermute | solution.py:25
  37.1 30.1 %collective-permute-start.3 = (bf16[704,256]{1,0:T(8,128)(2,1)S(1)}, bf16[704,256]{1,0:T(8,128)(2,1)S(1)}, u32[]{:S(2)}, u32[]{:S(2)}) collective-permute-start(bf16[704,256]{1,0:T(8,128)(2,1)S(1)} %bitcast.11), channel_id=1, source_target_pairs={{0,1},{1,0},{2,3},{3,2},{4,5},{5,4},{6,7},{7,6},{8,9},{9,8},{10,11... | collective-permute-start | bytes 1081352 | tf_op jit(solution)/shard_map/ppermute | solution.py:25
  37.2 30.0 %collective-permute-start.4 = (bf16[704,256]{1,0:T(8,128)(2,1)S(1)}, bf16[704,256]{1,0:T(8,128)(2,1)S(1)}, u32[]{:S(2)}, u32[]{:S(2)}) collective-permute-start(bf16[704,256]{1,0:T(8,128)(2,1)S(1)} %bitcast.13), channel_id=1, source_target_pairs={{0,1},{1,0},{2,3},{3,2},{4,5},{5,4},{6,7},{7,6},{8,9},{9,8},{10,11... | collective-permute-start | bytes 1081352 | tf_op jit(solution)/shard_map/ppermute | solution.py:25
  47.4 15.8 %all-to-all-start.2 = ((bf16[8,24,256]{2,1,0:T(8,128)(2,1)}), bf16[8,24,256]{2,1,0:T(8,128)(2,1)S(1)}, u32[]{:S(2)}, u32[]{:S(2)}) async-start(bf16[8,24,256]{2,1,0:T(8,128)(2,1)} %shard_map.102), calls=%async_computation.2 | async-start | bytes 196608 | tf_op jit(solution)/shard_map/all_to_all | solution.py:21
  63.8 10.9 %all-to-all-start.3 = ((bf16[8,24,256]{2,1,0:T(8,128)(2,1)}), bf16[8,24,256]{2,1,0:T(8,128)(2,1)S(1)}, u32[]{:S(2)}, u32[]{:S(2)}) async-start(bf16[8,24,256]{2,1,0:T(8,128)(2,1)} %get-tuple-element.8), calls=%async_computation.3 | async-start | bytes 196608 | tf_op jit(solution)/shard_map/all_to_all | solution.py:21
  92.6 4.7 %copy-start.6 = (bf16[704,256]{1,0:T(8,128)(2,1)S(1)}, bf16[704,256]{1,0:T(8,128)(2,1)}, u32[]{:S(2)}) copy-start(bf16[704,256]{1,0:T(8,128)(2,1)} %own.3) | copy-start | bytes 1081348
  93.7 12.9 %all-to-all-start.5 = ((bf16[16,24,704]{2,1,0:T(8,128)(2,1)}), bf16[16,24,704]{2,1,0:T(8,128)(2,1)S(1)}, u32[]{:S(2)}, u32[]{:S(2)}) async-start(bf16[16,24,704]{2,1,0:T(8,128)(2,1)} %shard_map.105), calls=%async_computation.5 | async-start | bytes 1179648 | tf_op jit(solution)/shard_map/all_to_all | solution.py:21
  97.3 44.5 %copy-start.8 = (bf16[256]{0:T(256)(128)(2,1)S(1)}, bf16[256]{0:T(256)(128)(2,1)}, u32[]{:S(2)}) copy-start(bf16[256]{0:T(256)(128)(2,1)} %param.19) | copy-start | bytes 1540
  97.3 6.9 %collective-permute-start.5 = (bf16[704,256]{1,0:T(8,128)(2,1)S(1)}, bf16[704,256]{1,0:T(8,128)(2,1)S(1)}, u32[]{:S(2)}, u32[]{:S(2)}) collective-permute-start(bf16[704,256]{1,0:T(8,128)(2,1)S(1)} %copy-done.6), channel_id=1, source_target_pairs={{0,1},{1,0},{2,3},{3,2},{4,5},{5,4},{6,7},{7,6},{8,9},{9,8},{10,11... | collective-permute-start | bytes 1081352 | tf_op jit(solution)/shard_map/ppermute | solution.py:25
  127.5 10.0 %collective-permute-start.6 = (bf16[192,256]{1,0:T(8,128)(2,1)S(1)}, bf16[192,256]{1,0:T(8,128)(2,1)S(1)}, u32[]{:S(2)}, u32[]{:S(2)}) collective-permute-start(bf16[192,256]{1,0:T(8,128)(2,1)S(1)} %bitcast.15), channel_id=1, source_target_pairs={{0,1},{1,0},{2,3},{3,2},{4,5},{5,4},{6,7},{7,6},{8,9},{9,8},{10,11... | collective-permute-start | bytes 294920 | tf_op jit(solution)/shard_map/ppermute | solution.py:25
  138.3 9.9 %all-to-all-start.8 = ((f32[16,1,384]{2,1,0:T(1,128)}), f32[16,1,384]{2,1,0:T(1,128)S(1)}, u32[]{:S(2)}, u32[]{:S(2)}) async-start(f32[16,1,384]{2,1,0:T(1,128)} %broadcast_in_dim.16), calls=%async_computation.8 | async-start | bytes 49152 | tf_op jit(solution)/shard_map/all_to_all | solution.py:21

commit v3 on v2

v3 whole, which is shorter than its diff:
```python
import functools

import jax
import jax.numpy as jnp
from jax import lax
from jax.experimental import pallas as pl
from jax.experimental.pallas import tpu as pltpu
from jax.sharding import Mesh
from jax.sharding import PartitionSpec as P

norm_eps = 1e-06
residual_weight = 0.25
branch_weight = 0.5
bf16 = jnp.bfloat16
f32 = jnp.float32
TILE = 8
HALF = TILE // 2
LANES = 128


def exchange(blocks, axis):
    return lax.all_to_all(blocks, axis, 0, 0, tiled=True)


def partner(value):
    return lax.ppermute(value, "c", [(0, 1), (1, 0)])


def rolled(value):
    return pltpu.roll(value, HALF, value.ndim - 2)


def first_half(shape):
    return lax.broadcasted_iota(jnp.int32, shape, len(shape) - 2) < HALF


def sum_of(parts):
    total = parts[0].astype(f32)
    for k in range(1, parts.shape[0]):
        total = total + parts[k].astype(f32)
    return total


def row_of(gain):
    gain = gain[...].astype(f32)
    return jnp.concatenate([gain[k : k + 1] for k in range(gain.shape[0])], axis=1)


def sums_of(x, gain, both):
    values = x[...].astype(f32)
    normed = (values * row_of(gain)).astype(bf16)
    return values, lax.dot_general(normed, both[...], (((1,), (1,)), ((), ())), preferred_element_type=f32)


def put_together(gate, up, both):
    hidden = gate.shape[0]
    both[:hidden] = gate[...]
    both[hidden:] = up[...]


def first_own_kernel(x, gain, gate, up, out, both, near, done):
    hidden = gate.shape[0]
    copies = [
        pltpu.make_async_copy(gain, near, done.at[2]),
        pltpu.make_async_copy(gate, both.at[:hidden], done.at[0]),
        pltpu.make_async_copy(up, both.at[hidden:], done.at[1]),
    ]
    for copy in copies:
        copy.start()
    for copy in copies:
        copy.wait()
    out[...] = sums_of(x, near, both)[1].astype(bf16)


def own_kernel(x, gain, gate, up, out, both):
    put_together(gate, up, both)
    out[...] = sums_of(x, gain, both)[1].astype(bf16)


def dealt(own, other, group):
    own = own.reshape(group // 2, TILE, own.shape[1])
    other = other.reshape(own.shape)
    first = first_half(own.shape)
    even = jnp.where(first, own, rolled(other))
    odd = jnp.where(first, rolled(own), other)
    return jnp.stack([even, odd], axis=1).reshape(group, TILE, own.shape[2])


def packed_kernel(group, x, gain, gate, up, own, *refs):
    out, both = refs[-2:]
    put_together(gate, up, both)
    values, other = sums_of(x, gain, both)
    own = own[...].astype(f32)
    whole = group * TILE
    count = own.shape[1] // LANES
    rest = dealt(own[whole:], other[whole:], group)
    own = own[:whole].reshape(group, TILE, count * LANES)
    other = other[:whole].reshape(own.shape)
    for k in range(count):
        lanes = slice(k * LANES, (k + 1) * LANES)
        out[:, k] = own[:, :, lanes].astype(bf16)
        out[:, count + k] = other[:, :, lanes].astype(bf16)
        out[:, 2 * count + k] = rest[:, :, lanes].astype(bf16)
    squares = jnp.sum(values * values, axis=1, keepdims=True)
    high = squares.astype(bf16).astype(f32)
    lane = lax.broadcasted_iota(jnp.int32, (values.shape[0], LANES), 1)
    squares = jnp.where(lane % 2 == 0, high, squares - high)
    rest = dealt(squares[whole:], squares[whole:], group)
    squares = squares[:whole].reshape(group, TILE, LANES)
    lane = lax.broadcasted_iota(jnp.int32, squares.shape, 2)
    out[:, 3 * count] = jnp.where(lane < 2, squares, rest).astype(bf16)


def hidden_kernel(features, parts, out):
    group, count = parts.shape[0], parts.shape[1] // 3
    hidden = out.shape[2]
    total = sum_of(parts)
    rows = jnp.concatenate(
        [jnp.concatenate([total[count * t + k] for k in range(count)], axis=1) for t in range(3)], axis=0
    )
    squares = total[3 * count]
    whole = squares[:, 0:1] + squares[:, 1:2]
    rest = squares[:, 2:3] + squares[:, 3:4]
    scale = lax.rsqrt(jnp.concatenate([whole, whole, rest], axis=0) / features + norm_eps)
    gate = rows[:, :hidden] * scale
    up = pltpu.roll(rows, hidden, 1)[:, :hidden] * scale
    rows = (gate * jax.nn.sigmoid(gate) * up).astype(bf16)
    for k in range(group):
        out[k] = rows


def down_kernel(hids, own, other, out):
    group = hids.shape[0]
    hidden, width = own.shape
    tiles = [
        hids[:, TILE * k : TILE * (k + 1)].astype(f32).reshape(group * TILE, hidden).astype(bf16) for k in range(3)
    ]
    dot = functools.partial(jnp.dot, preferred_element_type=f32)
    whole = dot(tiles[0], own[...]) + dot(tiles[1], other[...])
    mixed = dot(tiles[2], own[...]).reshape(group, TILE, width)
    mixed = mixed + rolled(dot(tiles[2], other[...]).reshape(group, TILE, width))
    mixed = mixed.reshape(group // 2, 2, TILE, width)
    even, odd = mixed[:, 0], mixed[:, 1]
    rest = jnp.where(first_half(even.shape), even, rolled(odd)).reshape(group // 2 * TILE, width)
    rows = jnp.concatenate([whole, rest], axis=0)
    out[...] = rows.reshape(out.shape).astype(bf16)


def updated(parts, start):
    return (residual_weight * start[...].astype(f32) + branch_weight * sum_of(parts)).astype(bf16)


def update_kernel(parts, start, out, kept):
    rows = updated(parts, start)
    kept[...] = rows
    for k in range(out.shape[0]):
        out[k] = rows


def last_kernel(parts, start, kept, out):
    rows = updated(parts, start)
    kept[...] = rows
    values = rows.astype(f32)
    squares = jnp.sum(values * values, axis=1, keepdims=True)
    lane = lax.broadcasted_iota(jnp.int32, (TILE, LANES), 1)
    tile = jnp.zeros((TILE, LANES), f32)
    for t in range(rows.shape[0] // TILE):
        tile = jnp.where(lane == t, squares[TILE * t : TILE * (t + 1)], tile)
    for k in range(out.shape[0]):
        out[k] = tile


def closing_kernel(features, squares, rows, gain, out):
    total = sum_of(squares)
    count = rows.shape[0] // TILE
    total = jnp.concatenate([total[:, t : t + 1] for t in range(count)], axis=0)
    scale = lax.rsqrt(total / features + norm_eps)
    closed = (rows[...].astype(f32) * scale * row_of(gain)).astype(bf16)
    for k in range(out.shape[0]):
        out[k] = closed


def kernel_call(kernel, outs, scratch=(), outside=()):
    inside = pl.BlockSpec(memory_space=pltpu.VMEM)
    anywhere = pl.BlockSpec(memory_space=pltpu.HBM)
    many = isinstance(outs, list)

    def call(*args):
        return pl.pallas_call(
            kernel,
            out_shape=outs,
            in_specs=[anywhere if k in outside else inside for k in range(len(args))],
            out_specs=[inside] * len(outs) if many else inside,
            scratch_shapes=scratch,
            compiler_params=pltpu.CompilerParams(vmem_limit_bytes=12 * 2**20),
        )(*args)

    return call


def half_step(layer, stream, start, gain, gates, ups, downs, features):
    ra, z = lax.axis_size("ra"), lax.axis_size("z")
    tokens, width = stream.shape
    hidden = gates[0].shape[0]
    room = [pltpu.VMEM((2 * hidden, width), bf16)]
    struct = jax.ShapeDtypeStruct
    sums = struct((tokens, 2 * hidden), bf16)
    near = pltpu.VMEM(gain.shape, bf16)
    if layer == 0:
        call = kernel_call(first_own_kernel, sums, [*room, near, pltpu.SemaphoreType.DMA((3,))], (1, 2, 3))
    else:
        call = kernel_call(own_kernel, sums, room)
    mine = (gain, gates[0], ups[0])
    if layer == 0:
        mine = [pltpu.with_memory_space_constraint(w, pltpu.HBM) for w in mine]
    own = call(stream, *mine)
    slots = 3 * (2 * hidden // LANES) + 1
    parts = kernel_call(
        functools.partial(packed_kernel, ra), struct((ra, slots, TILE, LANES), bf16), room
    )(stream, gain, gates[1], ups[1], own, start)
    parts = exchange(parts, "ra")
    hids = kernel_call(functools.partial(hidden_kernel, features), struct((ra, 3 * TILE, hidden), bf16))(parts)
    hids = exchange(hids, "ra")
    branch = kernel_call(down_kernel, struct((z, tokens // z, width), bf16))(hids, *downs)
    return exchange(branch, "z")


def body(
    hidden_states,
    gain_first,
    gate_first,
    up_first,
    down_first,
    gain_second,
    gate_second,
    up_second,
    down_second,
    gain_last,
):
    ra, z, c = (lax.axis_size(axis) for axis in ("ra", "z", "c"))
    width = hidden_states.shape[1]
    features = width * ra
    rows = hidden_states.shape[0] // (z * c)
    struct = jax.ShapeDtypeStruct
    blocks = hidden_states.reshape(z, c, rows, width)
    stream = lax.dynamic_index_in_dim(blocks, lax.axis_index("c"), 1, keepdims=False)
    start = lax.dynamic_index_in_dim(stream, lax.axis_index("z"), 0, keepdims=False)
    pairs = []
    for w in (gate_first.T, up_first.T, down_first, gate_second.T, up_second.T, down_second):
        pairs.append((w, partner(w)))
    gains = [gain.reshape(-1, LANES) for gain in (gain_first, gain_second, gain_last)]
    parts = half_step(0, stream.reshape(z * rows, width), start, gains[0], *pairs[:3], features)
    first, start = kernel_call(update_kernel, [struct((z, rows, width), bf16), struct((rows, width), bf16)])(
        parts, start
    )
    stream = exchange(first, "z").reshape(z * rows, width)
    parts = half_step(1, stream, start, gains[1], *pairs[3:], features)
    second, squares = kernel_call(
        last_kernel, [struct((rows, width), bf16), struct((ra, TILE, LANES), f32)]
    )(parts, start)
    squares = exchange(squares, "ra")
    closed = kernel_call(functools.partial(closing_kernel, features), struct((z * c, rows, width), bf16))(
        squares, second, gains[2]
    )
    return exchange(closed, ("z", "c")).reshape(hidden_states.shape)


def solution(mesh):
    split = Mesh(mesh.devices.reshape(mesh.shape["ra"], -1, 2), ("ra", "z", "c"))
    cb = ("z", "c")
    return jax.shard_map(
        body,
        mesh=split,
        in_specs=(
            P(None, "ra"),
            P("ra"),
            P("ra", cb),
            P("ra", cb),
            P(cb, "ra"),
            P("ra"),
            P("ra", cb),
            P("ra", cb),
            P(cb, "ra"),
            P("ra"),
        ),
        out_specs=P(None, "ra"),
        check_vma=False,
    )
```

time: 150 us -> 143 us (0.953)
  blocking collectives: 60.1 us -> 105 us
  waiting for transfers between devices: 36.1 us -> 11.6 us
  starting transfers between devices: 42.2 us -> 19 us
  local copies, waits for them, and re-layouts: 3.3 us -> 0.73 us
    all_to_all x4 -> x7, blocking collectives: 60.1 us -> 105 us  [exchange(): return lax.all_to_all(blocks, axis, 0, 0, tiled=True)]
    all_to_all x5 -> x2, waiting for transfers between devices: 31.7 us -> 9.09 us  [exchange(): return lax.all_to_all(blocks, axis, 0, 0, tiled=True)]
    all_to_all x5 -> x2, starting transfers between devices: 22.2 us -> 7.16 us  [exchange(): return lax.all_to_all(blocks, axis, 0, 0, tiled=True)]
    ppermute x7 -> x6, starting transfers between devices: 20 us -> 11.9 us  [partner(): return lax.ppermute(value, 'c', [(0, 1), (1, 0)])]
    ppermute x7 -> x6, waiting for transfers between devices: 4.39 us -> 2.53 us  [partner(): return lax.ppermute(value, 'c', [(0, 1), (1, 0)])]
    pallas_call x8 -> x11, Pallas kernels: 6.26 us -> 6.01 us  [call(): pl.pallas_call(kernel, out_shape=outs, in_specs=[anywhere if k in outside...]
  transfers between devices with their start and end apart: 12 -> 8, of which waited for: 10 -> 5; matrix products, arithmetic and copies ran while one was open for 0% -> 0% of each run, Pallas kernels for 1% -> 2%
where the time goes in v3:
time: 143 us; the launch traced here: 142 us
  blocking collectives  105 us (73%)
  starting transfers between devices  19 us (13%)
  waiting for transfers between devices  11.6 us (8%)
  Pallas kernels  6.01 us (4%)
    all_to_all x7, blocking collectives, exchange(): return lax.all_to_all(blocks, axis, 0, 0, tiled=True)  105 us
    ppermute x6, starting transfers between devices, partner(): return lax.ppermute(value, 'c', [(0, 1), (1, 0)])  11.9 us
    all_to_all x2, waiting for transfers between devices, exchange(): return lax.all_to_all(blocks, axis, 0, 0, tiled=True)  9.09 us
    all_to_all x2, starting transfers between devices, exchange(): return lax.all_to_all(blocks, axis, 0, 0, tiled=True)  7.16 us
    pallas_call x11, Pallas kernels, call(): pl.pallas_call(kernel, out_shape=outs, in_specs=[anywhere if k in outside...  6.01 us
  transfers between devices with their start and end apart: 8, of which 5 were waited for; matrix products, arithmetic and copies ran while one was open for 0% of the time, Pallas kernels for 2%

profile of v3, /device:TPU:1, one launch (start us, length us, event | category | flops | bytes accessed | tf_op | source)
XLA Modules:
  0.0 142.2 jit_solution(9254208785667987788)
XLA Ops:
  0.0 0.0 copy-start
  0.0 0.0 copy-start.5
  0.0 3.2 %collective-permute-start = (bf16[704,256]{1,0:T(8,128)(2,1)}, bf16[704,256]{1,0:T(8,128)(2,1)S(1)}, u32[]{:S(2)}, u32[]{:S(2)}) collective-permute-start(bf16[704,256]{1,0:T(8,128)(2,1)} %bitcast.29), channel_id=1, source_target_pairs={{0,1},{1,0},{2,3},{3,2},{4,5},{5,4},{6,7},{7,6},{8,9},{9,8},{10,11... | collective-permute-start | bytes 1081352 | tf_op jit(solution)/shard_map/ppermute | solution.py:26
  3.2 0.0 collective-permute-start.1
  3.2 0.0 copy-done
  3.2 1.5 %shard_map.100.own = bf16[192,1408]{1,0:T(8,128)(2,1)S(1)} custom-call(bf16[192,256]{1,0:T(8,128)(2,1)S(1)} %bitcast.15, bf16[2,128]{1,0:T(2,128)(2,1)} %bitcast.23, bf16[704,256]{1,0:T(8,128)(2,1)} %bitcast.30, bf16[704,256]{1,0:T(8,128)(2,1)} %bitcast.32), custom_call_target="tpu_custom_call" | custom-call | tf_op jit(solution)/shard_map/pallas_call | solution.py:189
  4.8 0.0 collective-permute-done.gate
  4.8 0.4 collective-permute-done.1.up
  5.2 0.0 copy-done.5
  5.2 0.4 shard_map.101
  5.7 21.8 %all_to_all.45.parts = bf16[16,34,8,128]{3,2,1,0:T(8,128)(2,1)S(1)} all-to-all(bf16[16,34,8,128]{3,2,1,0:T(8,128)(2,1)S(1)} %shard_map.101), channel_id=1, replica_groups=mesh['ra'=16,'z'=8,'c'=2] {'ra'}, dimensions={0} | all-to-all | bytes 2228224 | tf_op jit(solution)/shard_map/all_to_all | solution.py:22
  27.5 0.0 copy-start.1
  27.5 0.0 copy-start.2
  27.5 1.1 shard_map.102
  28.5 3.6 %all-to-all-start.1 = ((bf16[16,24,704]{2,1,0:T(8,128)(2,1)}), bf16[16,24,704]{2,1,0:T(8,128)(2,1)S(1)}, u32[]{:S(2)}, u32[]{:S(2)}) async-start(bf16[16,24,704]{2,1,0:T(8,128)(2,1)} %shard_map.102), calls=%async_computation.1 | async-start | bytes 1179648 | tf_op jit(solution)/shard_map/all_to_all | solution.py:22
  32.1 0.0 copy-done.1
  32.1 0.0 copy-start.6
  32.2 2.0 %collective-permute-start.2 = (bf16[704,256]{1,0:T(8,128)(2,1)S(1)}, bf16[704,256]{1,0:T(8,128)(2,1)S(1)}, u32[]{:S(2)}, u32[]{:S(2)}) collective-permute-start(bf16[704,256]{1,0:T(8,128)(2,1)S(1)} %copy-done.1), channel_id=1, source_target_pairs={{0,1},{1,0},{2,3},{3,2},{4,5},{5,4},{6,7},{7,6},{8,9},{9,8},{10,11... | collective-permute-start | bytes 1081352 | tf_op jit(solution)/shard_map/ppermute | solution.py:26
  34.1 0.0 copy-done.2
  34.1 0.1 collective-permute-start.3
  34.3 0.0 copy-done.3
  34.3 0.4 collective-permute-start.4
  34.7 0.8 collective-permute-done.2.other
  35.4 7.3 %all-to-all-done.1.hids = bf16[16,24,704]{2,1,0:T(8,128)(2,1)S(1)} async-done(((bf16[16,24,704]{2,1,0:T(8,128)(2,1)}), bf16[16,24,704]{2,1,0:T(8,128)(2,1)S(1)}, u32[]{:S(2)}, u32[]{:S(2)}) %all-to-all-start.1) | async-done | bytes 540704 | tf_op jit(solution)/shard_map/all_to_all | solution.py:22
  42.7 0.4 shard_map.103
  43.1 15.7 %all_to_all.46.parts = bf16[8,24,256]{2,1,0:T(8,128)(2,1)S(1)} all-to-all(bf16[8,24,256]{2,1,0:T(8,128)(2,1)S(1)} %shard_map.103), channel_id=1, replica_groups=mesh['ra'=16,'z'=8,'c'=2] {'z'}, dimensions={0} | all-to-all | bytes 196608 | tf_op jit(solution)/shard_map/all_to_all | solution.py:22
  58.8 10.0 %all_to_all.47 = bf16[8,24,256]{2,1,0:T(8,128)(2,1)S(1)} all-to-all(bf16[8,24,256]{2,1,0:T(8,128)(2,1)S(1)} %get-tuple-element.9), channel_id=1, replica_groups=mesh['ra'=16,'z'=8,'c'=2] {'z'}, dimensions={0} | all-to-all | bytes 196608 | tf_op jit(solution)/shard_map/all_to_all | solution.py:22
  68.7 0.0 copy-done.6
  68.7 0.4 shard_map.105.own
  69.1 0.0 collective-permute-done.3.gate
  69.2 0.0 collective-permute-done.4.up
  69.2 0.4 shard_map.106
  69.6 15.7 %all_to_all.48.parts = bf16[16,34,8,128]{3,2,1,0:T(8,128)(2,1)S(1)} all-to-all(bf16[16,34,8,128]{3,2,1,0:T(8,128)(2,1)S(1)} %shard_map.106), channel_id=1, replica_groups=mesh['ra'=16,'z'=8,'c'=2] {'ra'}, dimensions={0} | all-to-all | bytes 2228224 | tf_op jit(solution)/shard_map/all_to_all | solution.py:22
  85.3 1.1 shard_map.107
  86.4 3.6 %all-to-all-start.5 = ((bf16[16,24,704]{2,1,0:T(8,128)(2,1)}), bf16[16,24,704]{2,1,0:T(8,128)(2,1)S(1)}, u32[]{:S(2)}, u32[]{:S(2)}) async-start(bf16[16,24,704]{2,1,0:T(8,128)(2,1)} %shard_map.107), calls=%async_computation.5 | async-start | bytes 1179648 | tf_op jit(solution)/shard_map/all_to_all | solution.py:22
  90.0 0.0 copy-done.4
  90.0 0.0 copy-start.7
  90.0 6.2 %collective-permute-start.5 = (bf16[704,256]{1,0:T(8,128)(2,1)S(1)}, bf16[704,256]{1,0:T(8,128)(2,1)S(1)}, u32[]{:S(2)}, u32[]{:S(2)}) collective-permute-start(bf16[704,256]{1,0:T(8,128)(2,1)S(1)} %copy-done.4), channel_id=1, source_target_pairs={{0,1},{1,0},{2,3},{3,2},{4,5},{5,4},{6,7},{7,6},{8,9},{9,8},{10,11... | collective-permute-start | bytes 1081352 | tf_op jit(solution)/shard_map/ppermute | solution.py:26
  96.1 1.3 collective-permute-done.5.other
  97.4 1.8 %all-to-all-done.5.hids = bf16[16,24,704]{2,1,0:T(8,128)(2,1)S(1)} async-done(((bf16[16,24,704]{2,1,0:T(8,128)(2,1)}), bf16[16,24,704]{2,1,0:T(8,128)(2,1)S(1)}, u32[]{:S(2)}, u32[]{:S(2)}) %all-to-all-start.5) | async-done | bytes 540704 | tf_op jit(solution)/shard_map/all_to_all | solution.py:22
  99.3 0.4 shard_map.108
  99.6 10.0 %all_to_all.49.parts = bf16[8,24,256]{2,1,0:T(8,128)(2,1)S(1)} all-to-all(bf16[8,24,256]{2,1,0:T(8,128)(2,1)S(1)} %shard_map.108), channel_id=1, replica_groups=mesh['ra'=16,'z'=8,'c'=2] {'z'}, dimensions={0} | all-to-all | bytes 196608 | tf_op jit(solution)/shard_map/all_to_all | solution.py:22
  109.6 0.1 shard_map.109
  109.7 11.4 %all_to_all.50.squares = f32[16,8,128]{2,1,0:T(8,128)S(1)} all-to-all(f32[16,8,128]{2,1,0:T(8,128)S(1)} %get-tuple-element.11), channel_id=1, replica_groups=mesh['ra'=16,'z'=8,'c'=2] {'ra'}, dimensions={0} | all-to-all | bytes 131072 | tf_op jit(solution)/shard_map/all_to_all | solution.py:22
  121.1 0.0 copy-done.7
  121.1 0.2 shard_map.110
  121.2 20.3 %all_to_all.51 = bf16[16,24,256]{2,1,0:T(8,128)(2,1)S(1)} all-to-all(bf16[16,24,256]{2,1,0:T(8,128)(2,1)S(1)} %shard_map.110), channel_id=1, replica_groups=mesh['ra'=16,'z'=8,'c'=2] {'z','c'}, dimensions={0} | all-to-all | bytes 393216 | tf_op jit(solution)/shard_map/all_to_all | solution.py:22
  141.6 0.7 copy.12
  (5 shorter events, 0.0 us)
Async XLA Ops:
  0.0 3.2 %copy-start = (bf16[384,256]{1,0:T(8,128)(2,1)S(1)}, bf16[384,256]{1,0:T(8,128)(2,1)}, u32[]{:S(2)}) copy-start(bf16[384,256]{1,0:T(8,128)(2,1)} %param.10) | copy-start | bytes 589828
  0.0 5.2 %copy-start.5 = (bf16[256]{0:T(256)(128)(2,1)S(1)}, bf16[256]{0:T(256)(128)(2,1)}, u32[]{:S(2)}) copy-start(bf16[256]{0:T(256)(128)(2,1)} %param.11) | copy-start | bytes 1540
  0.0 4.8 %collective-permute-start = (bf16[704,256]{1,0:T(8,128)(2,1)}, bf16[704,256]{1,0:T(8,128)(2,1)S(1)}, u32[]{:S(2)}, u32[]{:S(2)}) collective-permute-start(bf16[704,256]{1,0:T(8,128)(2,1)} %bitcast.29), channel_id=1, source_target_pairs={{0,1},{1,0},{2,3},{3,2},{4,5},{5,4},{6,7},{7,6},{8,9},{9,8},{10,11... | collective-permute-start | bytes 1081352 | tf_op jit(solution)/shard_map/ppermute | solution.py:26
  3.2 2.0 %collective-permute-start.1 = (bf16[704,256]{1,0:T(8,128)(2,1)}, bf16[704,256]{1,0:T(8,128)(2,1)S(1)}, u32[]{:S(2)}, u32[]{:S(2)}) collective-permute-start(bf16[704,256]{1,0:T(8,128)(2,1)} %bitcast.31), channel_id=1, source_target_pairs={{0,1},{1,0},{2,3},{3,2},{4,5},{5,4},{6,7},{7,6},{8,9},{9,8},{10,11... | collective-permute-start | bytes 1081352 | tf_op jit(solution)/shard_map/ppermute | solution.py:26
  27.5 4.7 %copy-start.1 = (bf16[704,256]{1,0:T(8,128)(2,1)S(1)}, bf16[704,256]{1,0:T(8,128)(2,1)}, u32[]{:S(2)}) copy-start(bf16[704,256]{1,0:T(8,128)(2,1)} %own.2) | copy-start | bytes 1081348
  27.5 6.7 %copy-start.2 = (bf16[256,704]{0,1:T(8,128)(2,1)S(1)}, bf16[256,704]{0,1:T(8,128)(2,1)}, u32[]{:S(2)}) copy-start(bf16[256,704]{0,1:T(8,128)(2,1)} %param.16) | copy-start | bytes 1081348
  27.5 6.8 %copy-start.3 = (bf16[256,704]{0,1:T(8,128)(2,1)S(1)}, bf16[256,704]{0,1:T(8,128)(2,1)}, u32[]{:S(2)}) copy-start(bf16[256,704]{0,1:T(8,128)(2,1)} %param.17) | copy-start | bytes 1081348
  28.5 14.2 %all-to-all-start.1 = ((bf16[16,24,704]{2,1,0:T(8,128)(2,1)}), bf16[16,24,704]{2,1,0:T(8,128)(2,1)S(1)}, u32[]{:S(2)}, u32[]{:S(2)}) async-start(bf16[16,24,704]{2,1,0:T(8,128)(2,1)} %shard_map.102), calls=%async_computation.1 | async-start | bytes 1179648 | tf_op jit(solution)/shard_map/all_to_all | solution.py:22
  32.1 36.6 %copy-start.6 = (bf16[256]{0:T(256)(128)(2,1)S(1)}, bf16[256]{0:T(256)(128)(2,1)}, u32[]{:S(2)}) copy-start(bf16[256]{0:T(256)(128)(2,1)} %param.15) | copy-start | bytes 1540
  32.2 3.3 %collective-permute-start.2 = (bf16[704,256]{1,0:T(8,128)(2,1)S(1)}, bf16[704,256]{1,0:T(8,128)(2,1)S(1)}, u32[]{:S(2)}, u32[]{:S(2)}) collective-permute-start(bf16[704,256]{1,0:T(8,128)(2,1)S(1)} %copy-done.1), channel_id=1, source_target_pairs={{0,1},{1,0},{2,3},{3,2},{4,5},{5,4},{6,7},{7,6},{8,9},{9,8},{10,11... | collective-permute-start | bytes 1081352 | tf_op jit(solution)/shard_map/ppermute | solution.py:26
  34.1 35.0 %collective-permute-start.3 = (bf16[704,256]{1,0:T(8,128)(2,1)S(1)}, bf16[704,256]{1,0:T(8,128)(2,1)S(1)}, u32[]{:S(2)}, u32[]{:S(2)}) collective-permute-start(bf16[704,256]{1,0:T(8,128)(2,1)S(1)} %bitcast.19), channel_id=1, source_target_pairs={{0,1},{1,0},{2,3},{3,2},{4,5},{5,4},{6,7},{7,6},{8,9},{9,8},{10,11... | collective-permute-start | bytes 1081352 | tf_op jit(solution)/shard_map/ppermute | solution.py:26
  34.3 34.9 %collective-permute-start.4 = (bf16[704,256]{1,0:T(8,128)(2,1)S(1)}, bf16[704,256]{1,0:T(8,128)(2,1)S(1)}, u32[]{:S(2)}, u32[]{:S(2)}) collective-permute-start(bf16[704,256]{1,0:T(8,128)(2,1)S(1)} %bitcast.21), channel_id=1, source_target_pairs={{0,1},{1,0},{2,3},{3,2},{4,5},{5,4},{6,7},{7,6},{8,9},{9,8},{10,11... | collective-permute-start | bytes 1081352 | tf_op jit(solution)/shard_map/ppermute | solution.py:26
  85.3 4.7 %copy-start.4 = (bf16[704,256]{1,0:T(8,128)(2,1)S(1)}, bf16[704,256]{1,0:T(8,128)(2,1)}, u32[]{:S(2)}) copy-start(bf16[704,256]{1,0:T(8,128)(2,1)} %own.3) | copy-start | bytes 1081348
  86.4 12.9 %all-to-all-start.5 = ((bf16[16,24,704]{2,1,0:T(8,128)(2,1)}), bf16[16,24,704]{2,1,0:T(8,128)(2,1)S(1)}, u32[]{:S(2)}, u32[]{:S(2)}) async-start(bf16[16,24,704]{2,1,0:T(8,128)(2,1)} %shard_map.107), calls=%async_computation.5 | async-start | bytes 1179648 | tf_op jit(solution)/shard_map/all_to_all | solution.py:22
  90.0 31.1 %copy-start.7 = (bf16[256]{0:T(256)(128)(2,1)S(1)}, bf16[256]{0:T(256)(128)(2,1)}, u32[]{:S(2)}) copy-start(bf16[256]{0:T(256)(128)(2,1)} %param.19) | copy-start | bytes 1540
  90.0 7.5 %collective-permute-start.5 = (bf16[704,256]{1,0:T(8,128)(2,1)S(1)}, bf16[704,256]{1,0:T(8,128)(2,1)S(1)}, u32[]{:S(2)}, u32[]{:S(2)}) collective-permute-start(bf16[704,256]{1,0:T(8,128)(2,1)S(1)} %copy-done.4), channel_id=1, source_target_pairs={{0,1},{1,0},{2,3},{3,2},{4,5},{5,4},{6,7},{7,6},{8,9},{9,8},{10,11... | collective-permute-start | bytes 1081352 | tf_op jit(solution)/shard_map/ppermute | solution.py:26
